TPU v7x, 32 devices: a whole 2x2x4 slice. The times are simulated.
32 devices in a mesh: tp: 8 (over z, y), dp: 4 (over x, core).
Axes of the slice: x: 2, y: 2, z: 4, core: 2. Of those that a mesh axis runs over, the one named last changes fastest.
Arguments:
- stream: bfloat16 [128, 4096], P(None, ('dp', 'tp')), may hold values from -16 to 16
- lengths: int32 [128], P('dp'), may hold values from 1 to 64, 1024 in all
- prior_state: float32 [2, 128, 4096], P(None, 'dp', 'tp'), may hold values from -6 to 6
- prior_window: bfloat16 [2, 128, 3, 4096], P(None, 'dp', None, 'tp'), may hold values from -6 to 6
- norm_gain: float32 [2, 4096], P(None, 'dp'), may hold values from 0.1 to 1.9
- w_branch: bfloat16 [2, 4096, 4096], P(None, 'dp', 'tp'), may hold values from -0.09375 to 0.09375
- w_gate_branch: bfloat16 [2, 4096, 4096], P(None, 'dp', 'tp'), may hold values from -0.09375 to 0.09375
- conv_taps: bfloat16 [2, 4, 4096], P(None, None, 'tp'), may hold values from -3 to 3
- w_in_gate: bfloat16 [2, 256, 4096], P(None, None, 'tp'), may hold values from -0.375 to 0.375
- w_rec_gate: bfloat16 [2, 256, 4096], P(None, None, 'tp'), may hold values from -0.375 to 0.375
- decay_param: float32 [2, 4096], P(None, 'tp'), may hold values from -1 to 4
- w_out: bfloat16 [2, 4096, 4096], P(None, 'tp', 'dp'), may hold values from -0.1875 to 0.1875
Outputs:
- mixed_out: bfloat16 [128, 4096], P(None, ('dp', 'tp'))
- new_state: float32 [2, 128, 4096], P(None, 'dp', 'tp')
- new_window: bfloat16 [2, 128, 3, 4096], P(None, 'dp', None, 'tp')
All inputs are finite; a program needn't handle non-finite values. No bound on the sum of `lengths` on one device may be relied on, other than what follows from the above.
Results may differ from a plain program's by a relative error of at most 0.014.
Values may be sent and summed in bfloat16 or wider, within the bound.
A program may use at most 64 MiB of HBM per device.

v0:
```python
import functools

import jax
import jax.numpy as jnp
from jax import lax
from jax.experimental import pallas as pl
from jax.experimental.pallas import tpu as pltpu
from jax.sharding import PartitionSpec as P

D = 4096
BLOCK = 256


epsilon = 1e-06


def from_partner(block, axis, apart):
    count = lax.axis_size(axis)
    route = []
    for low in range(count):
        high = low | 1 << apart
        if high != low and high < count:
            route += [(low, high), (high, low)]
    return lax.ppermute(block, axis, route)


def norm_rows(block_rows, gain_values, squares):
    scaling = lax.rsqrt(squares / D + epsilon)
    return (block_rows.astype(jnp.float32) * scaling * gain_values).astype(jnp.bfloat16)


def normed_input(stream_local, gain_block):
    own_width = stream_local.shape[1]
    offset = lax.axis_index("tp") * own_width
    widened = stream_local.astype(jnp.float32)
    squares = lax.psum(jnp.sum(widened * widened, axis=1, keepdims=True), ("tp", "dp"))
    own_gain = lax.dynamic_slice_in_dim(gain_block, offset, own_width, 0)
    result = lax.all_gather(norm_rows(stream_local, own_gain, squares), "tp", axis=1, tiled=True)
    return result


def peer_block(convolved):
    col_count = convolved.shape[1]
    group_size = max(BLOCK // col_count, 1)
    device = lax.axis_index("tp")
    grouped = convolved
    for bit_number in range(group_size.bit_length() - 1):
        partner = from_partner(grouped, "tp", bit_number)
        is_upper = device // (1 << bit_number) % 2 == 1
        grouped = jnp.where(
            is_upper,
            jnp.concatenate([partner, grouped], axis=1),
            jnp.concatenate([grouped, partner], axis=1),
        )
    return grouped


def block_gates(grouped, weight):
    row_count = grouped.shape[0]
    col_count = weight.shape[1]
    blocks = max(col_count // BLOCK, 1)
    block_cols = min(col_count, BLOCK)
    inputs = grouped.reshape(row_count, blocks, BLOCK)
    tables = weight.reshape(BLOCK, blocks, block_cols)
    mapped = jnp.einsum("rnk,knc->rnc", inputs, tables, preferred_element_type=jnp.float32)
    return mapped.reshape(row_count, col_count)


def recurrent_step(
    normed,
    lengths,
    prior_state,
    prior_window,
    w_branch,
    w_gate_branch,
    conv_taps,
    w_in_gate,
    w_rec_gate,
    decay_param,
    w_out,
    stream_local,
):
    col_count = w_branch.shape[1]
    summed = lax.psum_scatter(
        jnp.concatenate(
            [
                jnp.dot(normed, w_branch, preferred_element_type=jnp.float32),
                jnp.dot(normed, w_gate_branch, preferred_element_type=jnp.float32),
            ],
            axis=1,
        ).astype(jnp.bfloat16),
        "dp",
        scatter_dimension=0,
        tiled=True,
    ).astype(jnp.float32)
    branch = summed[:, :col_count].astype(jnp.bfloat16)
    gate_in = summed[:, col_count:].astype(jnp.bfloat16)
    depth = prior_window.shape[1]
    needed = depth + 1 - jnp.arange(depth, dtype=jnp.int32)
    living = lengths[:, None, None] >= needed[None, :, None]
    history = jnp.where(living, prior_window, jnp.zeros_like(prior_window))
    window = jnp.concatenate([history, branch[:, None, :]], axis=1)
    convolved = jnp.sum(
        window.astype(jnp.float32) * conv_taps.astype(jnp.float32)[None], axis=1
    ).astype(jnp.bfloat16)
    grouped = peer_block(convolved)
    input_gate = jax.nn.sigmoid(block_gates(grouped, w_in_gate))
    recur_gate = jax.nn.sigmoid(block_gates(grouped, w_rec_gate))
    log_keep = 8.0 * recur_gate * jax.nn.log_sigmoid(decay_param)
    keeping = jnp.exp(log_keep)
    feeding = jnp.sqrt(-jnp.expm1(2.0 * log_keep))
    earlier = jnp.where(lengths[:, None] >= 2, prior_state, jnp.zeros_like(prior_state))
    state = keeping * earlier + feeding * input_gate * convolved.astype(jnp.float32)
    readout = (state * jax.nn.gelu(gate_in.astype(jnp.float32))).astype(jnp.bfloat16)
    mixed = jnp.dot(
        lax.all_gather(readout, "dp", axis=0, tiled=True), w_out, preferred_element_type=jnp.float32
    )
    own_width = stream_local.shape[1]
    offset = lax.axis_index("tp") * own_width
    own_cols = lax.dynamic_slice_in_dim(mixed, offset, own_width, 1) + stream_local.astype(
        jnp.float32
    )
    terms = lax.dynamic_update_slice_in_dim(mixed, own_cols, offset, 1)
    return (terms, state, window[:, 1:])


def body(
    stream,
    lengths,
    prior_state,
    prior_window,
    norm_gain,
    w_branch,
    w_gate_branch,
    conv_taps,
    w_in_gate,
    w_rec_gate,
    decay_param,
    w_out,
):
    normed = normed_input(stream, norm_gain[0])
    terms, state_first, window_first = recurrent_step(
        normed,
        lengths,
        prior_state[0],
        prior_window[0],
        w_branch[0],
        w_gate_branch[0],
        conv_taps[0],
        w_in_gate[0],
        w_rec_gate[0],
        decay_param[0],
        w_out[0],
        stream,
    )
    carried = lax.psum(terms, "tp").astype(jnp.bfloat16)
    widened = carried.astype(jnp.float32)
    squares = lax.psum(jnp.sum(widened * widened, axis=1, keepdims=True), "dp")
    normed = norm_rows(carried, norm_gain[1], squares)
    own_width = stream.shape[1]
    first = lax.dynamic_slice_in_dim(carried, lax.axis_index("tp") * own_width, own_width, 1)
    terms, state_second, window_second = recurrent_step(
        normed,
        lengths,
        prior_state[1],
        prior_window[1],
        w_branch[1],
        w_gate_branch[1],
        conv_taps[1],
        w_in_gate[1],
        w_rec_gate[1],
        decay_param[1],
        w_out[1],
        first,
    )
    second = lax.psum_scatter(terms, "tp", scatter_dimension=1, tiled=True).astype(jnp.bfloat16)
    return (
        second,
        jnp.stack([state_first, state_second]),
        jnp.stack([window_first, window_second]),
    )


HALVES = 4
MAIN_VMEM = 60 * 1024 * 1024
TAIL_VMEM = 4 * 1024 * 1024
MESH = pl.DeviceIdType.MESH


def negative_expm1(z):
    series = -z * (1.0 + z / 2.0 * (1.0 + z / 3.0 * (1.0 + z / 4.0 * (1.0 + z / 5.0))))
    return jnp.where(z > -0.1, series, 1.0 - jnp.exp(z))


def fused_kernel(
    nt,
    nd,
    halves,
    stream,
    lengths,
    prior_state,
    prior_window,
    norm_gain,
    w_branch,
    w_gate_branch,
    conv_taps,
    w_in_gate,
    w_rec_gate,
    decay_param,
    w_out,
    mixed_out,
    new_state,
    new_window,
    xg,
    part,
    pr,
    ro,
    rg,
    mx,
    ms,
    len_v,
    state_v,
    win_v,
    gain_v,
    wp_v,
    taps_v,
    gates_v,
    decay_v,
    wo_v,
    state_o,
    win_o,
    mix_o,
    in_sem,
    out_sem,
    xs,
    xr,
    ps,
    prs,
    gs,
    gr,
    ms_s,
    ms_r,
):
    t = lax.axis_index("tp")
    d = lax.axis_index("dp")
    layers = w_branch.shape[0]
    rows, own = stream.shape[1], stream.shape[2]
    r = rows // halves
    cols = w_branch.shape[2]
    width = w_branch.shape[1]

    barrier = pltpu.get_barrier_semaphore()
    tp_peers = [lax.rem(t + k, nt) for k in range(1, nt)]
    dp_peers = [lax.rem(d + k, nd) for k in range(1, nd)]
    for peer in tp_peers:
        pl.semaphore_signal(barrier, inc=1, device_id={"tp": peer}, device_id_type=MESH)
    for peer in dp_peers:
        pl.semaphore_signal(barrier, inc=1, device_id={"dp": peer}, device_id_type=MESH)

    counter = [0]

    def load(src, dst):
        copy = pltpu.make_async_copy(src, dst, in_sem.at[counter[0]])
        counter[0] += 1
        copy.start()
        return copy

    c_stream = load(stream, xg.at[0, t])
    c_gain = load(norm_gain, gain_v)
    c_len = load(lengths, len_v)
    loads = []
    for l in range(layers):
        c_w = [load(w_branch.at[l], wp_v.at[l, 0]), load(w_gate_branch.at[l], wp_v.at[l, 1])]
        c_s = [
            load(prior_window.at[l], win_v.at[l]),
            load(prior_state.at[l], state_v.at[l]),
            load(w_in_gate.at[l], gates_v.at[l, 0]),
            load(w_rec_gate.at[l], gates_v.at[l, 1]),
        ]
        if l == 0:
            c_s += [load(conv_taps, taps_v), load(decay_param, decay_v), c_len]
        c_o = [load(w_out.at[l], wo_v.at[l])]
        loads.append((c_w, c_s, c_o))

    sends = []

    def send(src, dst, ssem, rsem, axis, peer):
        copy = pltpu.make_async_remote_copy(
            src_ref=src,
            dst_ref=dst,
            send_sem=ssem,
            recv_sem=rsem,
            device_id={axis: peer},
            device_id_type=MESH,
        )
        copy.start()
        sends.append(copy)

    def arrived(dst, ssem, rsem, axis, peer):
        pltpu.make_async_remote_copy(
            src_ref=dst,
            dst_ref=dst,
            send_sem=ssem,
            recv_sem=rsem,
            device_id={axis: peer},
            device_id_type=MESH,
        ).wait_recv()

    def cut(h):
        return slice(h * r, (h + 1) * r)

    def send_features(l, h):
        for k, peer in enumerate(tp_peers):
            block = xg.at[l, t, :, pl.ds(h * r, r), :]
            send(block, block, xs.at[l, h, k], xr.at[l, h, t], "tp", peer)

    def project(l, h):
        for k, peer in enumerate(tp_peers):
            block = xg.at[l, peer, :, pl.ds(h * r, r), :]
            arrived(block, xs.at[l, h, k], xr.at[l, h, peer], "tp", peer)
        if h == 0:
            if l == 0:
                c_gain.wait()
            for copy in loads[l][0]:
                copy.wait()
        squares = jnp.zeros((nd * r, own), jnp.float32)
        pieces = []
        for j in range(nt):
            x = xg[l, j, :, cut(h), :].reshape(nd * r, own).astype(jnp.float32)
            squares = squares + x * x
            gain = gain_v[l : l + 1, j * own : (j + 1) * own]
            pieces.append((x * gain).astype(jnp.bfloat16))
        normed = jnp.concatenate(pieces, axis=1)
        total = jnp.sum(squares, axis=1, keepdims=True)
        high = total.astype(jnp.bfloat16).astype(jnp.float32)
        lane = lax.broadcasted_iota(jnp.int32, (nd * r, 128), 1)
        both = jnp.where(lane < 64, high, total - high).astype(jnp.bfloat16)
        part[l, h, :, :, 2 * cols :] = both.reshape(nd, r, 128)
        for w in range(2):
            product = jnp.dot(normed, wp_v[l, w], preferred_element_type=jnp.float32)
            part[l, h, :, :, w * cols : (w + 1) * cols] = product.astype(jnp.bfloat16).reshape(
                nd, r, cols
            )
        for k, peer in enumerate(dp_peers):
            send(
                part.at[l, h, peer],
                pr.at[l, h, d],
                ps.at[l, h, k],
                prs.at[l, h, d],
                "dp",
                peer,
            )

    def recur(l, h):
        summed = part[l, h, d].astype(jnp.float32)
        if h == 0:
            for copy in loads[l][1]:
                copy.wait()
        length = jnp.sum(
            jnp.where(
                lax.broadcasted_iota(jnp.int32, (r, rows), 0) + h * r
                == lax.broadcasted_iota(jnp.int32, (r, rows), 1),
                jnp.broadcast_to(len_v[...].astype(jnp.float32), (r, rows)),
                0.0,
            ),
            axis=1,
            keepdims=True,
        )
        depth = prior_window.shape[1]
        history = []
        for m in range(depth):
            row = win_v[l, m, cut(h), :].astype(jnp.float32)
            history.append(jnp.where(length >= depth + 1 - m, row, 0.0))
        taps = taps_v[l].astype(jnp.float32)
        before = history[0] * taps[0:1]
        for m in range(1, depth):
            before = before + history[m] * taps[m : m + 1]
        raw = decay_v[l : l + 1]
        log_decay = jnp.minimum(raw, 0.0) - jnp.log1p(jnp.exp(-jnp.abs(raw)))
        earlier = jnp.where(length >= 2, state_v[l, cut(h), :], 0.0)

        for k, peer in enumerate(dp_peers):
            arrived(pr.at[l, h, peer], ps.at[l, h, k], prs.at[l, h, peer], "dp", peer)
        for peer in dp_peers:
            summed = summed + pr[l, h, peer].astype(jnp.float32)
        squares = summed[:, 2 * cols : 2 * cols + 1] + summed[:, 2 * cols + 64 : 2 * cols + 65]
        scaling = lax.rsqrt(squares / (width * nd) + epsilon)
        branch = (summed[:, :cols] * scaling).astype(jnp.bfloat16)
        gate_in = (summed[:, cols : 2 * cols] * scaling).astype(jnp.bfloat16)
        for m in range(1, depth):
            win_o[l, m - 1, cut(h), :] = history[m].astype(jnp.bfloat16)
        win_o[l, depth - 1, cut(h), :] = branch
        convolved = (before + branch.astype(jnp.float32) * taps[depth : depth + 1]).astype(
            jnp.bfloat16
        )
        mapped = []
        for w in range(2):
            mapped.append(
                jnp.concatenate(
                    [
                        jnp.dot(
                            convolved[:, n * BLOCK : (n + 1) * BLOCK],
                            gates_v[l, w, :, n * BLOCK : (n + 1) * BLOCK],
                            preferred_element_type=jnp.float32,
                        )
                        for n in range(cols // BLOCK)
                    ],
                    axis=1,
                )
            )
        input_gate = jax.nn.sigmoid(mapped[0])
        recur_gate = jax.nn.sigmoid(mapped[1])
        log_keep = 8.0 * recur_gate * log_decay
        feeding = jnp.sqrt(negative_expm1(2.0 * log_keep))
        state = jnp.exp(log_keep) * earlier + feeding * input_gate * convolved.astype(jnp.float32)
        state_o[l, cut(h), :] = state
        ro[l, h] = (state * jax.nn.gelu(gate_in.astype(jnp.float32))).astype(jnp.bfloat16)
        for k, peer in enumerate(dp_peers):
            send(ro.at[l, h], rg.at[l, h, d], gs.at[l, h, k], gr.at[l, h, d], "dp", peer)
        rg[l, h, d] = ro[l, h]

    def mix(l, h):
        if h == 0:
            for copy in loads[l][2]:
                copy.wait()
        for k, peer in enumerate(dp_peers):
            arrived(rg.at[l, h, peer], gs.at[l, h, k], gr.at[l, h, peer], "dp", peer)
        readout = rg[l, h].reshape(nd * r, cols)
        mixed = jnp.dot(readout, wo_v[l], preferred_element_type=jnp.float32)
        for j in range(nt):
            mx[l, h, j] = mixed[:, j * own : (j + 1) * own].astype(jnp.bfloat16)
        for k, peer in enumerate(tp_peers):
            send(mx.at[l, h, peer], ms.at[l, h, t], ms_s.at[l, h, k], ms_r.at[l, h, t], "tp", peer)

    def collect(l, h):
        total = mx[l, h, t].astype(jnp.float32)
        total = total + xg[l, t, :, cut(h), :].reshape(nd * r, own).astype(jnp.float32)
        for k, peer in enumerate(tp_peers):
            arrived(ms.at[l, h, peer], ms_s.at[l, h, k], ms_r.at[l, h, peer], "tp", peer)
            total = total + ms[l, h, peer].astype(jnp.float32)
        result = total.astype(jnp.bfloat16).reshape(nd, r, own)
        if l + 1 < layers:
            xg[l + 1, t, :, cut(h), :] = result
            send_features(l + 1, h)
        else:
            mix_o[:, cut(h), :] = result

    stores = []

    def store(src, dst):
        copy = pltpu.make_async_copy(src, dst, out_sem.at[len(stores)])
        copy.start()
        stores.append(copy)

    c_stream.wait()
    pl.semaphore_wait(barrier, nt - 1 + nd - 1)
    for h in range(halves):
        send_features(0, h)
    for l in range(layers):
        for h in range(halves):
            project(l, h)
        for h in range(halves):
            recur(l, h)
        for h in range(halves):
            mix(l, h)
        store(state_o.at[l], new_state.at[l])
        store(win_o.at[l], new_window.at[l])
        for h in range(halves):
            collect(l, h)
    store(mix_o, mixed_out)
    for copy in sends:
        copy.wait_send()
    for copy in stores:
        copy.wait()


def tail_kernel(mixed, state, window, mixed_out, state_out, window_out, a, b, c, in_sem, out_sem):
    triples = ((mixed, a, mixed_out), (state, b, state_out), (window, c, window_out))
    loads = []
    for k, (src, held, _) in enumerate(triples):
        loads.append(pltpu.make_async_copy(src, held, in_sem.at[k]))
        loads[-1].start()
    stores = []
    for k, (_, held, dst) in enumerate(triples):
        loads[k].wait()
        stores.append(pltpu.make_async_copy(held, dst, out_sem.at[k]))
        stores[-1].start()
    for copy in stores:
        copy.wait()


def fused(
    nt,
    nd,
    halves,
    stream,
    lengths,
    prior_state,
    prior_window,
    norm_gain,
    w_branch,
    w_gate_branch,
    conv_taps,
    w_in_gate,
    w_rec_gate,
    decay_param,
    w_out,
):
    layers, width, cols = w_branch.shape
    batch, own = stream.shape
    rows = batch // nd
    r = rows // halves
    depth = prior_window.shape[2]
    window = prior_window.transpose(0, 2, 1, 3)
    bf16, f32 = jnp.bfloat16, jnp.float32
    anywhere = pl.BlockSpec(memory_space=pl.ANY)
    dma = pltpu.SemaphoreType.DMA
    mixed, state, new_window = pl.pallas_call(
        functools.partial(fused_kernel, nt, nd, halves),
        out_shape=(
            jax.ShapeDtypeStruct((nd, rows, own), bf16),
            jax.ShapeDtypeStruct(prior_state.shape, f32),
            jax.ShapeDtypeStruct(window.shape, bf16),
        ),
        in_specs=[pl.BlockSpec(memory_space=pltpu.HBM)] * 12,
        out_specs=(anywhere,) * 3,
        scratch_shapes=[
            pltpu.VMEM((layers, nt, nd, rows, own), bf16),
            pltpu.VMEM((layers, halves, nd, r, 2 * cols + 128), bf16),
            pltpu.VMEM((layers, halves, nd, r, 2 * cols + 128), bf16),
            pltpu.VMEM((layers, halves, r, cols), bf16),
            pltpu.VMEM((layers, halves, nd, r, cols), bf16),
            pltpu.VMEM((layers, halves, nt, nd * r, own), bf16),
            pltpu.VMEM((layers, halves, nt, nd * r, own), bf16),
            pltpu.VMEM((1, rows), jnp.int32),
            pltpu.VMEM(prior_state.shape, f32),
            pltpu.VMEM(window.shape, bf16),
            pltpu.VMEM(norm_gain.shape, f32),
            pltpu.VMEM((layers, 2, width, cols), bf16),
            pltpu.VMEM(conv_taps.shape, bf16),
            pltpu.VMEM((layers, 2, BLOCK, cols), bf16),
            pltpu.VMEM(decay_param.shape, f32),
            pltpu.VMEM(w_out.shape, bf16),
            pltpu.VMEM(prior_state.shape, f32),
            pltpu.VMEM(window.shape, bf16),
            pltpu.VMEM((nd, rows, own), bf16),
            dma((5 + 7 * layers,)),
            dma((2 * layers + 1,)),
            dma((layers, halves, nt)),
            dma((layers, halves, nt)),
            dma((layers, halves, nd)),
            dma((layers, halves, nd)),
            dma((layers, halves, nd)),
            dma((layers, halves, nd)),
            dma((layers, halves, nt)),
            dma((layers, halves, nt)),
        ],
        compiler_params=pltpu.CompilerParams(collective_id=0, has_side_effects=True, vmem_limit_bytes=MAIN_VMEM),
    )(
        stream.reshape(nd, rows, own),
        lengths.reshape(1, rows),
        prior_state,
        window,
        norm_gain,
        w_branch,
        w_gate_branch,
        conv_taps,
        w_in_gate,
        w_rec_gate,
        decay_param,
        w_out,
    )
    finals = (mixed, state, new_window)
    mixed, state, new_window = pl.pallas_call(
        tail_kernel,
        out_shape=tuple(jax.ShapeDtypeStruct(a.shape, a.dtype) for a in finals),
        in_specs=[anywhere] * 3,
        out_specs=(anywhere,) * 3,
        scratch_shapes=[pltpu.VMEM(a.shape, a.dtype) for a in finals] + [dma((3,)), dma((3,))],
        compiler_params=pltpu.CompilerParams(vmem_limit_bytes=TAIL_VMEM),
    )(*finals)
    return mixed.reshape(batch, own), state, new_window.transpose(0, 2, 1, 3)


def step(nt, nd, *arrays):
    stream, w_branch = arrays[0], arrays[5]
    rows, cols = stream.shape[0] // nd, w_branch.shape[2]
    if cols % BLOCK == 0 and stream.shape[1] % 128 == 0 and rows % (8 * HALVES) == 0:
        return fused(nt, nd, HALVES, *arrays)
    return body(*arrays)


def solution(mesh):
    placed = (
        P(None, ("dp", "tp")),
        P("dp"),
        P(None, "dp", "tp"),
        P(None, "dp", None, "tp"),
        P(None, "dp"),
        P(None, "dp", "tp"),
        P(None, "dp", "tp"),
        P(None, None, "tp"),
        P(None, None, "tp"),
        P(None, None, "tp"),
        P(None, "tp"),
        P(None, "tp", "dp"),
    )
    return jax.shard_map(
        functools.partial(step, mesh.shape["tp"], mesh.shape["dp"]),
        mesh=mesh,
        in_specs=placed,
        out_specs=(P(None, ("dp", "tp")), P(None, "dp", "tp"), P(None, "dp", None, "tp")),
        check_vma=False,
    )
```

profile of v0, /device:TPU:0, one launch (start us, length us, event | category | flops | bytes accessed | tf_op | source)
XLA Modules:
  0.0 51.9 jit_solution(12831364921762667709)
XLA Ops:
  0.6 47.4 %shard_map.139 = (bf16[4,32,128]{2,1,0:T(8,128)(2,1)}, f32[2,32,512]{2,1,0:T(8,128)}, bf16[2,3,32,512]{3,2,1,0:T(8,128)(2,1)}) custom-call(bf16[4,32,128]{2,1,0:T(8,128)(2,1)} %bitcast.6, s32[1,32]{1,0:T(1,128)} %bitcast.7, f32[2,32,512]{2,1,0:T(8,128)} %prior_state.1, bf16[2,3,32,512]{3,2,1,0:T(8,128)(2,1)} %bitcast.5, f32[2,1024]{1,0:T(2,128)} %norm_gain.1, ...), custom_call_target="tpu_custom_call" | custom-call | tf_op jit(solution)/shard_map/pallas_call | solution.py:518
  48.1 0.0 copy-start
  48.1 0.9 %copy-done = bf16[2,3,32,512]{3,2,1,0:T(8,128)(2,1)S(1)} copy-done((bf16[2,3,32,512]{3,2,1,0:T(8,128)(2,1)S(1)}, bf16[2,3,32,512]{3,2,1,0:T(8,128)(2,1)}, u32[]{:S(2)}) %copy-start) | copy-done | bytes 196632
  49.0 0.0 copy-start.1
  49.0 0.9 %copy-done.1 = f32[2,32,512]{2,1,0:T(8,128)S(1)} copy-done((f32[2,32,512]{2,1,0:T(8,128)S(1)}, f32[2,32,512]{2,1,0:T(8,128)}, u32[]{:S(2)}) %copy-start.1) | copy-done | bytes 131096
  49.9 0.0 copy-start.2
  49.9 0.8 %copy-done.2 = bf16[4,32,128]{2,1,0:T(8,128)(2,1)S(1)} copy-done((bf16[4,32,128]{2,1,0:T(8,128)(2,1)S(1)}, bf16[4,32,128]{2,1,0:T(8,128)(2,1)}, u32[]{:S(2)}) %copy-start.2) | copy-done | bytes 32792
  50.7 1.2 %shard_map.140 = (bf16[4,32,128]{2,1,0:T(8,128)(2,1)}, f32[2,32,512]{2,1,0:T(8,128)}, bf16[2,3,32,512]{3,2,1,0:T(8,128)(2,1)}) custom-call(bf16[4,32,128]{2,1,0:T(8,128)(2,1)S(1)} %copy-done.2, f32[2,32,512]{2,1,0:T(8,128)S(1)} %copy-done.1, bf16[2,3,32,512]{3,2,1,0:T(8,128)(2,1)S(1)} %copy-done), custom_call_target="tpu_custom_call" | custom-call | tf_op jit(solution)/shard_map/pallas_call | solution.py:574
Async XLA Ops:
  48.1 0.9 %copy-start = (bf16[2,3,32,512]{3,2,1,0:T(8,128)(2,1)S(1)}, bf16[2,3,32,512]{3,2,1,0:T(8,128)(2,1)}, u32[]{:S(2)}) copy-start(bf16[2,3,32,512]{3,2,1,0:T(8,128)(2,1)} %get-tuple-element.11.window) | copy-start | bytes 589828
  49.0 0.9 %copy-start.1 = (f32[2,32,512]{2,1,0:T(8,128)S(1)}, f32[2,32,512]{2,1,0:T(8,128)}, u32[]{:S(2)}) copy-start(f32[2,32,512]{2,1,0:T(8,128)} %get-tuple-element.10.state) | copy-start | bytes 393220
  49.9 0.8 %copy-start.2 = (bf16[4,32,128]{2,1,0:T(8,128)(2,1)S(1)}, bf16[4,32,128]{2,1,0:T(8,128)(2,1)}, u32[]{:S(2)}) copy-start(bf16[4,32,128]{2,1,0:T(8,128)(2,1)} %get-tuple-element.9.mixed) | copy-start | bytes 98308
where the time goes:
time: 52.1 us; the launch traced here: 51.9 us
  Pallas kernels  48.6 us (93%)
  local copies, waits for them, and re-layouts  2.58 us (5%)
  between operations  0.65 us (1%)
    pallas_call x1, Pallas kernels, fused(): pl.pallas_call(functools.partial(fused_kernel, nt, nd, halves), out_shape...  47.4 us
    unnamed x6, local copies, waits for them, and re-layouts  2.58 us
    pallas_call x1, Pallas kernels, fused(): pl.pallas_call(tail_kernel, out_shape=tuple((jax.ShapeDtypeStruct(a.shape...  1.21 us

commit v1 on v0

--- a/solution.py
+++ b/solution.py
@@ -208,16 +208,20 @@
     w_rec_gate,
     decay_param,
     w_out,
-    mixed_out,
-    new_state,
-    new_window,
+    mix_o,
+    state_o,
+    hist_o,
+    branch_o,
     xg,
     part,
     pr,
+    half,
+    px,
     ro,
     rg,
     mx,
     ms,
+    aux,
     len_v,
     state_v,
     win_v,
@@ -227,65 +231,67 @@
     gates_v,
     decay_v,
     wo_v,
-    state_o,
-    win_o,
-    mix_o,
     in_sem,
-    out_sem,
-    xs,
+    sent,
     xr,
-    ps,
-    prs,
-    gs,
+    pr_r,
+    px_r,
     gr,
-    ms_s,
     ms_r,
+    as_r,
 ):
     t = lax.axis_index("tp")
     d = lax.axis_index("dp")
+    side = d // 2
+    mate = d + 1 - 2 * lax.rem(d, 2)
+    across = lax.rem(d + 2, nd)
     layers = w_branch.shape[0]
     rows, own = stream.shape[1], stream.shape[2]
     r = rows // halves
     cols = w_branch.shape[2]
     width = w_branch.shape[1]
+    depth = prior_window.shape[1]
 
     barrier = pltpu.get_barrier_semaphore()
-    tp_peers = [lax.rem(t + k, nt) for k in range(1, nt)]
-    dp_peers = [lax.rem(d + k, nd) for k in range(1, nd)]
-    for peer in tp_peers:
+    tp_peers = [(k, flipped(t, k, nt)) for k in range(nt - 1, 0, -1)]
+    for _, peer in tp_peers:
         pl.semaphore_signal(barrier, inc=1, device_id={"tp": peer}, device_id_type=MESH)
-    for peer in dp_peers:
+    for peer in (across, mate):
         pl.semaphore_signal(barrier, inc=1, device_id={"dp": peer}, device_id_type=MESH)
 
     counter = [0]
 
-    def load(src, dst):
-        copy = pltpu.make_async_copy(src, dst, in_sem.at[counter[0]])
+    def load(*pairs):
+        sem = in_sem.at[counter[0]]
         counter[0] += 1
-        copy.start()
-        return copy
-
-    c_stream = load(stream, xg.at[0, t])
-    c_gain = load(norm_gain, gain_v)
-    c_len = load(lengths, len_v)
-    loads = []
+        for src, dst in pairs:
+            pltpu.make_async_copy(src, dst, sem).start()
+        return sem
+
+    def loaded(ref, sem):
+        pltpu.make_async_copy(ref, ref, sem).wait()
+
+    c_stream = load(*[(stream.at[block_of(d, s)], xg.at[0, t, s]) for s in range(nd)])
+    c_first = [
+        (held, load((src, held)))
+        for src, held in (
+            (lengths, len_v),
+            (conv_taps, taps_v),
+            (prior_window, win_v),
+            (prior_state, state_v),
+        )
+    ]
+    c_gain = load((norm_gain, gain_v))
+    c_w, c_o = [], []
     for l in range(layers):
-        c_w = [load(w_branch.at[l], wp_v.at[l, 0]), load(w_gate_branch.at[l], wp_v.at[l, 1])]
-        c_s = [
-            load(prior_window.at[l], win_v.at[l]),
-            load(prior_state.at[l], state_v.at[l]),
-            load(w_in_gate.at[l], gates_v.at[l, 0]),
-            load(w_rec_gate.at[l], gates_v.at[l, 1]),
-        ]
+        c_w.append(load((w_branch.at[l], wp_v.at[l, 0]), (w_gate_branch.at[l], wp_v.at[l, 1])))
         if l == 0:
-            c_s += [load(conv_taps, taps_v), load(decay_param, decay_v), c_len]
-        c_o = [load(w_out.at[l], wo_v.at[l])]
-        loads.append((c_w, c_s, c_o))
-
-    sends = []
-
-    def send(src, dst, ssem, rsem, axis, peer):
-        copy = pltpu.make_async_remote_copy(
+            c_gates = load((w_in_gate, gates_v.at[0]), (w_rec_gate, gates_v.at[1]))
+            c_decay = load((decay_param, decay_v))
+        c_o.append(load((w_out.at[l], wo_v.at[l])))
+
+    def remote(src, dst, ssem, rsem, axis, peer):
+        return pltpu.make_async_remote_copy(
             src_ref=src,
             dst_ref=dst,
             send_sem=ssem,
@@ -293,36 +299,57 @@
             device_id={axis: peer},
             device_id_type=MESH,
         )
-        copy.start()
-        sends.append(copy)
-
-    def arrived(dst, ssem, rsem, axis, peer):
-        pltpu.make_async_remote_copy(
-            src_ref=dst,
-            dst_ref=dst,
-            send_sem=ssem,
-            recv_sem=rsem,
-            device_id={axis: peer},
-            device_id_type=MESH,
-        ).wait_recv()
+
+    def send(src, dst, kind, rsem, axis, peer):
+        remote(src, dst, sent.at[kind], rsem, axis, peer).start()
+
+    def arrived(ref, rsem, axis, peer):
+        remote(ref, ref, sent.at[0], rsem, axis, peer).wait_recv()
+
+    def all_sent(ref, kind, axis, peer):
+        remote(ref, ref, sent.at[kind], sent.at[kind], axis, peer).wait_send()
 
     def cut(h):
         return slice(h * r, (h + 1) * r)
 
     def send_features(l, h):
-        for k, peer in enumerate(tp_peers):
-            block = xg.at[l, t, :, pl.ds(h * r, r), :]
-            send(block, block, xs.at[l, h, k], xr.at[l, h, t], "tp", peer)
+        block = xg.at[l, t, :, pl.ds(h * r, r), :]
+        for _, peer in tp_peers:
+            send(block, block, 0, xr.at[l, h], "tp", peer)
+
+    def prepare():
+        length = jnp.sum(
+            jnp.where(
+                lax.broadcasted_iota(jnp.int32, (rows, rows), 0)
+                == lax.broadcasted_iota(jnp.int32, (rows, rows), 1),
+                jnp.broadcast_to(len_v[...].astype(jnp.float32), (rows, rows)),
+                0.0,
+            ),
+            axis=1,
+            keepdims=True,
+        )
+        for l in range(layers):
+            taps = taps_v[l].astype(jnp.float32)
+            before = jnp.zeros((rows, cols), jnp.float32)
+            for m in range(depth):
+                row = win_v[l, m].astype(jnp.float32)
+                row = jnp.where(length >= depth + 1 - m, row, 0.0)
+                before = before + row * taps[m : m + 1]
+                if m > 0:
+                    hist_o[l, m - 1] = row.astype(jnp.bfloat16)
+            aux[l, side, 0] = before
+            aux[l, side, 1] = jnp.where(length >= 2, state_v[l], 0.0)
+
+    def send_history(l):
+        block = aux.at[l, side]
+        send(block, block, 5, as_r.at[l], "dp", across)
 
     def project(l, h):
-        for k, peer in enumerate(tp_peers):
-            block = xg.at[l, peer, :, pl.ds(h * r, r), :]
-            arrived(block, xs.at[l, h, k], xr.at[l, h, peer], "tp", peer)
+        arrived(xg.at[l, pl.ds(0, nt - 1), :, pl.ds(h * r, r), :], xr.at[l, h], "tp", tp_peers[0][1])
         if h == 0:
             if l == 0:
-                c_gain.wait()
-            for copy in loads[l][0]:
-                copy.wait()
+                loaded(gain_v, c_gain)
+            loaded(wp_v.at[l], c_w[l])
         squares = jnp.zeros((nd * r, own), jnp.float32)
         pieces = []
         for j in range(nt):
@@ -341,55 +368,34 @@
             part[l, h, :, :, w * cols : (w + 1) * cols] = product.astype(jnp.bfloat16).reshape(
                 nd, r, cols
             )
-        for k, peer in enumerate(dp_peers):
-            send(
-                part.at[l, h, peer],
-                pr.at[l, h, d],
-                ps.at[l, h, k],
-                prs.at[l, h, d],
-                "dp",
-                peer,
-            )
+        send(part.at[l, h, pl.ds(2, 2)], pr.at[l, h], 1, pr_r.at[l, h], "dp", mate)
+
+    def halve(l, h):
+        arrived(pr.at[l, h], pr_r.at[l, h], "dp", mate)
+        both = part[l, h, 0:2].astype(jnp.float32) + pr[l, h].astype(jnp.float32)
+        half[l, h] = both.astype(jnp.bfloat16)
+        send(half.at[l, h], px.at[l, h], 2, px_r.at[l, h], "dp", across)
 
     def recur(l, h):
-        summed = part[l, h, d].astype(jnp.float32)
         if h == 0:
-            for copy in loads[l][1]:
-                copy.wait()
-        length = jnp.sum(
-            jnp.where(
-                lax.broadcasted_iota(jnp.int32, (r, rows), 0) + h * r
-                == lax.broadcasted_iota(jnp.int32, (r, rows), 1),
-                jnp.broadcast_to(len_v[...].astype(jnp.float32), (r, rows)),
-                0.0,
-            ),
-            axis=1,
-            keepdims=True,
-        )
-        depth = prior_window.shape[1]
-        history = []
-        for m in range(depth):
-            row = win_v[l, m, cut(h), :].astype(jnp.float32)
-            history.append(jnp.where(length >= depth + 1 - m, row, 0.0))
+            if l == 0:
+                loaded(gates_v, c_gates)
+                loaded(decay_v, c_decay)
+            arrived(aux.at[l, 1 - side], as_r.at[l], "dp", across)
+        before = aux[l, :, 0, cut(h), :].reshape(2 * r, cols)
+        earlier = aux[l, :, 1, cut(h), :].reshape(2 * r, cols)
         taps = taps_v[l].astype(jnp.float32)
-        before = history[0] * taps[0:1]
-        for m in range(1, depth):
-            before = before + history[m] * taps[m : m + 1]
         raw = decay_v[l : l + 1]
         log_decay = jnp.minimum(raw, 0.0) - jnp.log1p(jnp.exp(-jnp.abs(raw)))
-        earlier = jnp.where(length >= 2, state_v[l, cut(h), :], 0.0)
-
-        for k, peer in enumerate(dp_peers):
-            arrived(pr.at[l, h, peer], ps.at[l, h, k], prs.at[l, h, peer], "dp", peer)
-        for peer in dp_peers:
-            summed = summed + pr[l, h, peer].astype(jnp.float32)
+
+        arrived(px.at[l, h], px_r.at[l, h], "dp", across)
+        summed = half[l, h].astype(jnp.float32) + px[l, h].astype(jnp.float32)
+        summed = summed.reshape(2 * r, 2 * cols + 128)
         squares = summed[:, 2 * cols : 2 * cols + 1] + summed[:, 2 * cols + 64 : 2 * cols + 65]
         scaling = lax.rsqrt(squares / (width * nd) + epsilon)
         branch = (summed[:, :cols] * scaling).astype(jnp.bfloat16)
         gate_in = (summed[:, cols : 2 * cols] * scaling).astype(jnp.bfloat16)
-        for m in range(1, depth):
-            win_o[l, m - 1, cut(h), :] = history[m].astype(jnp.bfloat16)
-        win_o[l, depth - 1, cut(h), :] = branch
+        branch_o[l, :, cut(h), :] = branch.reshape(2, r, cols)
         convolved = (before + branch.astype(jnp.float32) * taps[depth : depth + 1]).astype(
             jnp.bfloat16
         )
@@ -400,7 +406,7 @@
                     [
                         jnp.dot(
                             convolved[:, n * BLOCK : (n + 1) * BLOCK],
-                            gates_v[l, w, :, n * BLOCK : (n + 1) * BLOCK],
+                            gates_v[w, l, :, n * BLOCK : (n + 1) * BLOCK],
                             preferred_element_type=jnp.float32,
                         )
                         for n in range(cols // BLOCK)
@@ -413,31 +419,30 @@
         log_keep = 8.0 * recur_gate * log_decay
         feeding = jnp.sqrt(negative_expm1(2.0 * log_keep))
         state = jnp.exp(log_keep) * earlier + feeding * input_gate * convolved.astype(jnp.float32)
-        state_o[l, cut(h), :] = state
-        ro[l, h] = (state * jax.nn.gelu(gate_in.astype(jnp.float32))).astype(jnp.bfloat16)
-        for k, peer in enumerate(dp_peers):
-            send(ro.at[l, h], rg.at[l, h, d], gs.at[l, h, k], gr.at[l, h, d], "dp", peer)
-        rg[l, h, d] = ro[l, h]
+        state_o[l, :, cut(h), :] = state.reshape(2, r, cols)
+        readout = (state * jax.nn.gelu(gate_in.astype(jnp.float32))).astype(jnp.bfloat16)
+        ro[l, h] = readout.reshape(2, r, cols)
+        send(ro.at[l, h], rg.at[l, h], 3, gr.at[l, h], "dp", mate)
 
     def mix(l, h):
         if h == 0:
-            for copy in loads[l][2]:
-                copy.wait()
-        for k, peer in enumerate(dp_peers):
-            arrived(rg.at[l, h, peer], gs.at[l, h, k], gr.at[l, h, peer], "dp", peer)
-        readout = rg[l, h].reshape(nd * r, cols)
+            loaded(wo_v.at[l], c_o[l])
+        arrived(rg.at[l, h], gr.at[l, h], "dp", mate)
+        readout = jnp.concatenate(
+            [ro[l, h].reshape(2 * r, cols), rg[l, h].reshape(2 * r, cols)], axis=0
+        )
         mixed = jnp.dot(readout, wo_v[l], preferred_element_type=jnp.float32)
         for j in range(nt):
             mx[l, h, j] = mixed[:, j * own : (j + 1) * own].astype(jnp.bfloat16)
-        for k, peer in enumerate(tp_peers):
-            send(mx.at[l, h, peer], ms.at[l, h, t], ms_s.at[l, h, k], ms_r.at[l, h, t], "tp", peer)
+        for k, peer in tp_peers:
+            send(mx.at[l, h, peer], ms.at[l, h, k - 1], 4, ms_r.at[l, h], "tp", peer)
 
     def collect(l, h):
         total = mx[l, h, t].astype(jnp.float32)
         total = total + xg[l, t, :, cut(h), :].reshape(nd * r, own).astype(jnp.float32)
-        for k, peer in enumerate(tp_peers):
-            arrived(ms.at[l, h, peer], ms_s.at[l, h, k], ms_r.at[l, h, peer], "tp", peer)
-            total = total + ms[l, h, peer].astype(jnp.float32)
+        arrived(ms.at[l, h], ms_r.at[l, h], "tp", tp_peers[0][1])
+        for k in range(nt - 1):
+            total = total + ms[l, h, k].astype(jnp.float32)
         result = total.astype(jnp.bfloat16).reshape(nd, r, own)
         if l + 1 < layers:
             xg[l + 1, t, :, cut(h), :] = result
@@ -445,46 +450,61 @@
         else:
             mix_o[:, cut(h), :] = result
 
-    stores = []
-
-    def store(src, dst):
-        copy = pltpu.make_async_copy(src, dst, out_sem.at[len(stores)])
-        copy.start()
-        stores.append(copy)
-
-    c_stream.wait()
-    pl.semaphore_wait(barrier, nt - 1 + nd - 1)
+    loaded(xg.at[0, t], c_stream)
+    pl.semaphore_wait(barrier, nt - 1 + 2)
     for h in range(halves):
         send_features(0, h)
+    for ref, sem in c_first:
+        loaded(ref, sem)
+    prepare()
+    send_history(0)
     for l in range(layers):
         for h in range(halves):
             project(l, h)
+            if h > 0:
+                halve(l, h - 1)
+        halve(l, halves - 1)
         for h in range(halves):
             recur(l, h)
-        for h in range(halves):
-            mix(l, h)
-        store(state_o.at[l], new_state.at[l])
-        store(win_o.at[l], new_window.at[l])
+            if h > 0:
+                mix(l, h - 1)
+        mix(l, halves - 1)
+        if l + 1 < layers:
+            send_history(l + 1)
         for h in range(halves):
             collect(l, h)
-    store(mix_o, mixed_out)
-    for copy in sends:
-        copy.wait_send()
+    all_sent(xg.at[:, pl.ds(0, nt - 1)], 0, "tp", tp_peers[0][1])
+    all_sent(pr, 1, "dp", mate)
+    all_sent(px, 2, "dp", across)
+    all_sent(rg, 3, "dp", mate)
+    all_sent(ms, 4, "tp", tp_peers[0][1])
+    all_sent(aux.at[:, 0], 5, "dp", across)
+
+
+def flipped(index, mask, count):
+    for bit in range(count.bit_length() - 1):
+        if mask >> bit & 1:
+            index = index + (1 << bit) * (1 - 2 * (index // (1 << bit) % 2))
+    return index
+
+
+def block_of(d, s):
+    core = lax.rem(d, 2)
+    return 2 * (s % 2) + (core if s < 2 else 1 - core)
+
+
+def tail_kernel(mixed, state, hist, branch, mixed_out, state_out, window_out, sem):
+    d = lax.axis_index("dp")
+    side = d // 2
+    layers, depth = window_out.shape[:2]
+    pairs = [(mixed.at[s], mixed_out.at[block_of(d, s)]) for s in range(mixed.shape[0])]
+    for l in range(layers):
+        pairs.append((state.at[l, side], state_out.at[l]))
+        pairs.append((hist.at[l], window_out.at[l, pl.ds(0, depth - 1)]))
+        pairs.append((branch.at[l, side], window_out.at[l, depth - 1]))
+    stores = [pltpu.make_async_copy(src, dst, sem.at[k]) for k, (src, dst) in enumerate(pairs)]
     for copy in stores:
-        copy.wait()
-
-
-def tail_kernel(mixed, state, window, mixed_out, state_out, window_out, a, b, c, in_sem, out_sem):
-    triples = ((mixed, a, mixed_out), (state, b, state_out), (window, c, window_out))
-    loads = []
-    for k, (src, held, _) in enumerate(triples):
-        loads.append(pltpu.make_async_copy(src, held, in_sem.at[k]))
-        loads[-1].start()
-    stores = []
-    for k, (_, held, dst) in enumerate(triples):
-        loads[k].wait()
-        stores.append(pltpu.make_async_copy(held, dst, out_sem.at[k]))
-        stores[-1].start()
+        copy.start()
     for copy in stores:
         copy.wait()
 
@@ -514,48 +534,50 @@
     window = prior_window.transpose(0, 2, 1, 3)
     bf16, f32 = jnp.bfloat16, jnp.float32
     anywhere = pl.BlockSpec(memory_space=pl.ANY)
+    held = pl.BlockSpec(memory_space=pltpu.VMEM)
     dma = pltpu.SemaphoreType.DMA
-    mixed, state, new_window = pl.pallas_call(
+    finals = pl.pallas_call(
         functools.partial(fused_kernel, nt, nd, halves),
         out_shape=(
-            jax.ShapeDtypeStruct((nd, rows, own), bf16),
-            jax.ShapeDtypeStruct(prior_state.shape, f32),
-            jax.ShapeDtypeStruct(window.shape, bf16),
+            pltpu.VMEM((nd, rows, own), bf16),
+            pltpu.VMEM((layers, 2, rows, cols), f32),
+            pltpu.VMEM((layers, depth - 1, rows, cols), bf16),
+            pltpu.VMEM((layers, 2, rows, cols), bf16),
         ),
         in_specs=[pl.BlockSpec(memory_space=pltpu.HBM)] * 12,
-        out_specs=(anywhere,) * 3,
+        out_specs=(held,) * 4,
         scratch_shapes=[
             pltpu.VMEM((layers, nt, nd, rows, own), bf16),
             pltpu.VMEM((layers, halves, nd, r, 2 * cols + 128), bf16),
-            pltpu.VMEM((layers, halves, nd, r, 2 * cols + 128), bf16),
-            pltpu.VMEM((layers, halves, r, cols), bf16),
-            pltpu.VMEM((layers, halves, nd, r, cols), bf16),
+            pltpu.VMEM((layers, halves, 2, r, 2 * cols + 128), bf16),
+            pltpu.VMEM((layers, halves, 2, r, 2 * cols + 128), bf16),
+            pltpu.VMEM((layers, halves, 2, r, 2 * cols + 128), bf16),
+            pltpu.VMEM((layers, halves, 2, r, cols), bf16),
+            pltpu.VMEM((layers, halves, 2, r, cols), bf16),
             pltpu.VMEM((layers, halves, nt, nd * r, own), bf16),
-            pltpu.VMEM((layers, halves, nt, nd * r, own), bf16),
+            pltpu.VMEM((layers, halves, nt - 1, nd * r, own), bf16),
+            pltpu.VMEM((layers, 2, 2, rows, cols), f32),
             pltpu.VMEM((1, rows), jnp.int32),
             pltpu.VMEM(prior_state.shape, f32),
             pltpu.VMEM(window.shape, bf16),
             pltpu.VMEM(norm_gain.shape, f32),
             pltpu.VMEM((layers, 2, width, cols), bf16),
             pltpu.VMEM(conv_taps.shape, bf16),
-            pltpu.VMEM((layers, 2, BLOCK, cols), bf16),
+            pltpu.VMEM((2, layers, BLOCK, cols), bf16),
             pltpu.VMEM(decay_param.shape, f32),
             pltpu.VMEM(w_out.shape, bf16),
-            pltpu.VMEM(prior_state.shape, f32),
-            pltpu.VMEM(window.shape, bf16),
-            pltpu.VMEM((nd, rows, own), bf16),
-            dma((5 + 7 * layers,)),
-            dma((2 * layers + 1,)),
-            dma((layers, halves, nt)),
-            dma((layers, halves, nt)),
-            dma((layers, halves, nd)),
-            dma((layers, halves, nd)),
-            dma((layers, halves, nd)),
-            dma((layers, halves, nd)),
-            dma((layers, halves, nt)),
-            dma((layers, halves, nt)),
+            dma((8 + 2 * layers,)),
+            dma((6,)),
+            dma((layers, halves)),
+            dma((layers, halves)),
+            dma((layers, halves)),
+            dma((layers, halves)),
+            dma((layers, halves)),
+            dma((layers,)),
         ],
-        compiler_params=pltpu.CompilerParams(collective_id=0, has_side_effects=True, vmem_limit_bytes=MAIN_VMEM),
+        compiler_params=pltpu.CompilerParams(
+            collective_id=0, has_side_effects=True, vmem_limit_bytes=MAIN_VMEM
+        ),
     )(
         stream.reshape(nd, rows, own),
         lengths.reshape(1, rows),
@@ -570,13 +592,16 @@
         decay_param,
         w_out,
     )
-    finals = (mixed, state, new_window)
     mixed, state, new_window = pl.pallas_call(
         tail_kernel,
-        out_shape=tuple(jax.ShapeDtypeStruct(a.shape, a.dtype) for a in finals),
-        in_specs=[anywhere] * 3,
+        out_shape=(
+            jax.ShapeDtypeStruct((nd, rows, own), bf16),
+            jax.ShapeDtypeStruct(prior_state.shape, f32),
+            jax.ShapeDtypeStruct(window.shape, bf16),
+        ),
+        in_specs=[held] * 4,
         out_specs=(anywhere,) * 3,
-        scratch_shapes=[pltpu.VMEM(a.shape, a.dtype) for a in finals] + [dma((3,)), dma((3,))],
+        scratch_shapes=[dma((nd + 3 * layers,))],
         compiler_params=pltpu.CompilerParams(vmem_limit_bytes=TAIL_VMEM),
     )(*finals)
     return mixed.reshape(batch, own), state, new_window.transpose(0, 2, 1, 3)
@@ -585,7 +610,7 @@
 def step(nt, nd, *arrays):
     stream, w_branch = arrays[0], arrays[5]
     rows, cols = stream.shape[0] // nd, w_branch.shape[2]
-    if cols % BLOCK == 0 and stream.shape[1] % 128 == 0 and rows % (8 * HALVES) == 0:
+    if nd == 4 and nt & (nt - 1) == 0 and cols % BLOCK == 0 and stream.shape[1] % 128 == 0 and rows % (8 * HALVES) == 0:
         return fused(nt, nd, HALVES, *arrays)
     return body(*arrays)
 

time: 52.1 us -> 44.5 us (0.85)
  Pallas kernels: 48.6 us -> 43.6 us
  local copies, waits for them, and re-layouts: 2.58 us -> 0 us
    pallas_call x1, Pallas kernels: 47.4 us -> 42.8 us  [fused(): pl.pallas_call(functools.partial(fused_kernel, nt, nd, halves), out_shape...]
    unnamed x6 -> x0, local copies, waits for them, and re-layouts: 2.58 us -> none
where the time goes in v1:
time: 44.5 us; the launch traced here: 44.3 us
  Pallas kernels  43.6 us (98%)
  between operations  0.64 us (1%)
    pallas_call x1, Pallas kernels, fused(): pl.pallas_call(functools.partial(fused_kernel, nt, nd, halves), out_shape...  42.8 us

profile of v1, /device:TPU:0, one launch (start us, length us, event | category | flops | bytes accessed | tf_op | source)
XLA Modules:
  0.0 44.3 jit_solution(9924377933512047373)
XLA Ops:
  0.6 42.8 %shard_map.139 = (bf16[4,32,128]{2,1,0:T(8,128)(2,1)S(1)}, f32[2,2,32,512]{3,2,1,0:T(8,128)S(1)}, bf16[2,2,32,512]{3,2,1,0:T(8,128)(2,1)S(1)}, bf16[2,2,32,512]{3,2,1,0:T(8,128)(2,1)S(1)}) custom-call(bf16[4,32,128]{2,1,0:T(8,128)(2,1)} %bitcast.6, s32[1,32]{1,0:T(1,128)} %bitcast.7, f32[2,32,512]{2,1,0:T(8,128)} %prior_state.1, ...), custom_call_target="tpu_custom_call" | custom-call | tf_op jit(solution)/shard_map/pallas_call | solution.py:539
  43.5 0.8 %shard_map.140 = (bf16[4,32,128]{2,1,0:T(8,128)(2,1)}, f32[2,32,512]{2,1,0:T(8,128)}, bf16[2,3,32,512]{3,2,1,0:T(8,128)(2,1)}) custom-call(bf16[4,32,128]{2,1,0:T(8,128)(2,1)S(1)} %get-tuple-element.10.mixed, f32[2,2,32,512]{3,2,1,0:T(8,128)S(1)} %get-tuple-element.11.state, bf16[2,2,32,512]{3,2,1,0:T(8,128)(2,1)S(1)} %get-tuple-element.12.hist, ...), custom_call_target="tpu_custom_call" | custom-call | tf_op jit(solution)/shard_map/pallas_call | solution.py:595

commit v2 on v1

--- a/solution.py
+++ b/solution.py
@@ -181,7 +181,7 @@
     )
 
 
-HALVES = 4
+GROUPS = 2
 MAIN_VMEM = 60 * 1024 * 1024
 TAIL_VMEM = 4 * 1024 * 1024
 MESH = pl.DeviceIdType.MESH
@@ -195,7 +195,7 @@
 def fused_kernel(
     nt,
     nd,
-    halves,
+    groups,
     stream,
     lengths,
     prior_state,
@@ -210,17 +210,20 @@
     w_out,
     mix_o,
     state_o,
+    state_m,
     hist_o,
     branch_o,
+    branch_m,
     xg,
+    xm,
     part,
-    pr,
-    half,
     px,
-    ro,
-    rg,
     mx,
     ms,
+    fo,
+    fm,
+    res,
+    am,
     aux,
     len_v,
     state_v,
@@ -234,20 +237,29 @@
     in_sem,
     sent,
     xr,
-    pr_r,
+    xr_m,
     px_r,
-    gr,
     ms_r,
-    as_r,
+    f_r,
+    res_r,
+    aux_r,
+    wp_r,
+    wo_r,
+    gain_r,
+    st_r,
+    br_r,
 ):
     t = lax.axis_index("tp")
     d = lax.axis_index("dp")
-    side = d // 2
-    mate = d + 1 - 2 * lax.rem(d, 2)
+    core = lax.rem(d, 2)
+    mate = d + 1 - 2 * core
     across = lax.rem(d + 2, nd)
+    corner = lax.rem(mate + 2, nd)
     layers = w_branch.shape[0]
+    last = layers - 1
     rows, own = stream.shape[1], stream.shape[2]
-    r = rows // halves
+    r = rows // (2 * groups)
+    full = nd * r
     cols = w_branch.shape[2]
     width = w_branch.shape[1]
     depth = prior_window.shape[1]
@@ -255,8 +267,11 @@
     barrier = pltpu.get_barrier_semaphore()
     tp_peers = [(k, flipped(t, k, nt)) for k in range(nt - 1, 0, -1)]
     for _, peer in tp_peers:
-        pl.semaphore_signal(barrier, inc=1, device_id={"tp": peer}, device_id_type=MESH)
-    for peer in (across, mate):
+        for other in (d, mate):
+            pl.semaphore_signal(
+                barrier, inc=1, device_id={"tp": peer, "dp": other}, device_id_type=MESH
+            )
+    for peer in (across, corner, mate):
         pl.semaphore_signal(barrier, inc=1, device_id={"dp": peer}, device_id_type=MESH)
 
     counter = [0]
@@ -271,7 +286,13 @@
     def loaded(ref, sem):
         pltpu.make_async_copy(ref, ref, sem).wait()
 
-    c_stream = load(*[(stream.at[block_of(d, s)], xg.at[0, t, s]) for s in range(nd)])
+    def span(k, i):
+        side = core if k == 0 else 1 - core
+        return pl.ds(pl.multiple_of((side * groups + i) * r, r), r)
+
+    c_own = [load((stream.at[:, span(0, i), :], xg.at[0, i, t, 0])) for i in range(groups)]
+    c_mate = load(*[(stream.at[:, span(1, i), :], xm.at[i]) for i in range(groups)])
+    c_gain = load((norm_gain, gain_v.at[0]))
     c_first = [
         (held, load((src, held)))
         for src, held in (
@@ -281,41 +302,36 @@
             (prior_state, state_v),
         )
     ]
-    c_gain = load((norm_gain, gain_v))
     c_w, c_o = [], []
     for l in range(layers):
-        c_w.append(load((w_branch.at[l], wp_v.at[l, 0]), (w_gate_branch.at[l], wp_v.at[l, 1])))
+        c_w.append(load((w_branch.at[l], wp_v.at[l, 0, 0]), (w_gate_branch.at[l], wp_v.at[l, 0, 1])))
+        c_o.append(load((w_out.at[l], wo_v.at[l, 0])))
         if l == 0:
             c_gates = load((w_in_gate, gates_v.at[0]), (w_rec_gate, gates_v.at[1]))
             c_decay = load((decay_param, decay_v))
-        c_o.append(load((w_out.at[l], wo_v.at[l])))
-
-    def remote(src, dst, ssem, rsem, axis, peer):
+
+    kinds = {}
+
+    def remote(src, dst, ssem, rsem, where):
         return pltpu.make_async_remote_copy(
             src_ref=src,
             dst_ref=dst,
             send_sem=ssem,
             recv_sem=rsem,
-            device_id={axis: peer},
+            device_id=where,
             device_id_type=MESH,
         )
 
-    def send(src, dst, kind, rsem, axis, peer):
-        remote(src, dst, sent.at[kind], rsem, axis, peer).start()
-
-    def arrived(ref, rsem, axis, peer):
-        remote(ref, ref, sent.at[0], rsem, axis, peer).wait_recv()
-
-    def all_sent(ref, kind, axis, peer):
-        remote(ref, ref, sent.at[kind], sent.at[kind], axis, peer).wait_send()
-
-    def cut(h):
-        return slice(h * r, (h + 1) * r)
-
-    def send_features(l, h):
-        block = xg.at[l, t, :, pl.ds(h * r, r), :]
-        for _, peer in tp_peers:
-            send(block, block, 0, xr.at[l, h], "tp", peer)
+    def send(src, dst, kind, rsem, where):
+        ssem = sent.at[kinds.setdefault(kind, len(kinds))]
+        remote(src, dst, ssem, rsem, where).start()
+
+    def arrived(ref, rsem):
+        remote(ref, ref, sent.at[0], rsem, {"dp": mate}).wait_recv()
+
+    def all_sent(kind, ref):
+        sem = sent.at[kinds[kind]]
+        remote(ref, ref, sem, sem, {"dp": mate}).wait_send()
 
     def prepare():
         length = jnp.sum(
@@ -337,65 +353,76 @@
                 before = before + row * taps[m : m + 1]
                 if m > 0:
                     hist_o[l, m - 1] = row.astype(jnp.bfloat16)
-            aux[l, side, 0] = before
-            aux[l, side, 1] = jnp.where(length >= 2, state_v[l], 0.0)
+            earlier = jnp.where(length >= 2, state_v[l], 0.0)
+            for k in range(2):
+                for i in range(groups):
+                    piece = slice((k * groups + i) * r, (k * groups + i + 1) * r)
+                    am[l, k, i, 0] = before[piece]
+                    am[l, k, i, 1] = earlier[piece]
+            aux[l, d] = am[l, core]
 
     def send_history(l):
-        block = aux.at[l, side]
-        send(block, block, 5, as_r.at[l], "dp", across)
-
-    def project(l, h):
-        arrived(xg.at[l, pl.ds(0, nt - 1), :, pl.ds(h * r, r), :], xr.at[l, h], "tp", tp_peers[0][1])
-        if h == 0:
-            if l == 0:
-                loaded(gain_v, c_gain)
-            loaded(wp_v.at[l], c_w[l])
-        squares = jnp.zeros((nd * r, own), jnp.float32)
-        pieces = []
-        for j in range(nt):
-            x = xg[l, j, :, cut(h), :].reshape(nd * r, own).astype(jnp.float32)
-            squares = squares + x * x
-            gain = gain_v[l : l + 1, j * own : (j + 1) * own]
-            pieces.append((x * gain).astype(jnp.bfloat16))
-        normed = jnp.concatenate(pieces, axis=1)
+        send(am.at[l, core], aux.at[l, d], "aux", aux_r.at[l], {"dp": across})
+        send(am.at[l, 1 - core], aux.at[l, d], "aux", aux_r.at[l], {"dp": corner})
+        send(am.at[l, 1 - core], aux.at[l, d], "aux", aux_r.at[l], {"dp": mate})
+
+    def send_weights(l):
+        loaded(wp_v.at[l, 0], c_w[l])
+        send(wp_v.at[l, 0], wp_v.at[l, 1], "wp", wp_r.at[l], {"dp": mate})
+
+    def send_out(l):
+        loaded(wo_v.at[l, 0], c_o[l])
+        send(wo_v.at[l, 0], wo_v.at[l, 1], "wo", wo_r.at[l], {"dp": mate})
+
+    def project(l, i):
+        if l == 0:
+            arrived(xg.at[l, i, pl.ds(0, nt - 1), 0], xr.at[l, i])
+            arrived(xg.at[l, i, :, 1], xr_m.at[i])
+        else:
+            arrived(xg.at[l, i, pl.ds(0, nt - 1)], xr.at[l, i])
+        if i == 0 and l == 0:
+            arrived(gain_v.at[1], gain_r.at[0])
+        squares = jnp.zeros((full, own), jnp.float32)
+        products = [None, None]
+        for k in range(2):
+            pieces = []
+            for j in range(nt):
+                x = xg[l, i, j, k].reshape(full, own).astype(jnp.float32)
+                squares = squares + x * x
+                gain = gain_v[k, l : l + 1, j * own : (j + 1) * own]
+                pieces.append((x * gain).astype(jnp.bfloat16))
+            normed = jnp.concatenate(pieces, axis=1)
+            if i == 0 and k == 1:
+                arrived(wp_v.at[l, 1], wp_r.at[l])
+            for w in range(2):
+                term = jnp.dot(normed, wp_v[l, k, w], preferred_element_type=jnp.float32)
+                products[w] = term if k == 0 else products[w] + term
         total = jnp.sum(squares, axis=1, keepdims=True)
         high = total.astype(jnp.bfloat16).astype(jnp.float32)
-        lane = lax.broadcasted_iota(jnp.int32, (nd * r, 128), 1)
-        both = jnp.where(lane < 64, high, total - high).astype(jnp.bfloat16)
-        part[l, h, :, :, 2 * cols :] = both.reshape(nd, r, 128)
+        lane = lax.broadcasted_iota(jnp.int32, (full, 128), 1)
+        part[l, i, :, 2 * cols :] = jnp.where(lane < 64, high, total - high).astype(jnp.bfloat16)
         for w in range(2):
-            product = jnp.dot(normed, wp_v[l, w], preferred_element_type=jnp.float32)
-            part[l, h, :, :, w * cols : (w + 1) * cols] = product.astype(jnp.bfloat16).reshape(
-                nd, r, cols
-            )
-        send(part.at[l, h, pl.ds(2, 2)], pr.at[l, h], 1, pr_r.at[l, h], "dp", mate)
-
-    def halve(l, h):
-        arrived(pr.at[l, h], pr_r.at[l, h], "dp", mate)
-        both = part[l, h, 0:2].astype(jnp.float32) + pr[l, h].astype(jnp.float32)
-        half[l, h] = both.astype(jnp.bfloat16)
-        send(half.at[l, h], px.at[l, h], 2, px_r.at[l, h], "dp", across)
-
-    def recur(l, h):
-        if h == 0:
+            part[l, i, :, w * cols : (w + 1) * cols] = products[w].astype(jnp.bfloat16)
+        send(part.at[l, i], px.at[l, i], "px", px_r.at[l, i], {"dp": across})
+
+    def recur(l, i):
+        if i == 0:
             if l == 0:
                 loaded(gates_v, c_gates)
                 loaded(decay_v, c_decay)
-            arrived(aux.at[l, 1 - side], as_r.at[l], "dp", across)
-        before = aux[l, :, 0, cut(h), :].reshape(2 * r, cols)
-        earlier = aux[l, :, 1, cut(h), :].reshape(2 * r, cols)
+            arrived(aux.at[l, pl.ds(0, nd - 1)], aux_r.at[l])
+        before = aux[l, :, i, 0].reshape(full, cols)
+        earlier = aux[l, :, i, 1].reshape(full, cols)
         taps = taps_v[l].astype(jnp.float32)
         raw = decay_v[l : l + 1]
         log_decay = jnp.minimum(raw, 0.0) - jnp.log1p(jnp.exp(-jnp.abs(raw)))
-
-        arrived(px.at[l, h], px_r.at[l, h], "dp", across)
-        summed = half[l, h].astype(jnp.float32) + px[l, h].astype(jnp.float32)
-        summed = summed.reshape(2 * r, 2 * cols + 128)
+        arrived(px.at[l, i], px_r.at[l, i])
+        summed = part[l, i].astype(jnp.float32) + px[l, i].astype(jnp.float32)
         squares = summed[:, 2 * cols : 2 * cols + 1] + summed[:, 2 * cols + 64 : 2 * cols + 65]
         scaling = lax.rsqrt(squares / (width * nd) + epsilon)
         branch = (summed[:, :cols] * scaling).astype(jnp.bfloat16)
         gate_in = (summed[:, cols : 2 * cols] * scaling).astype(jnp.bfloat16)
-        branch_o[l, :, cut(h), :] = branch.reshape(2, r, cols)
+        branch_o[l, i] = branch.reshape(nd, r, cols)
         convolved = (before + branch.astype(jnp.float32) * taps[depth : depth + 1]).astype(
             jnp.bfloat16
         )
@@ -419,66 +446,112 @@
         log_keep = 8.0 * recur_gate * log_decay
         feeding = jnp.sqrt(negative_expm1(2.0 * log_keep))
         state = jnp.exp(log_keep) * earlier + feeding * input_gate * convolved.astype(jnp.float32)
-        state_o[l, :, cut(h), :] = state.reshape(2, r, cols)
+        state_o[l, i] = state.reshape(nd, r, cols)
         readout = (state * jax.nn.gelu(gate_in.astype(jnp.float32))).astype(jnp.bfloat16)
-        ro[l, h] = readout.reshape(2, r, cols)
-        send(ro.at[l, h], rg.at[l, h], 3, gr.at[l, h], "dp", mate)
-
-    def mix(l, h):
-        if h == 0:
-            loaded(wo_v.at[l], c_o[l])
-        arrived(rg.at[l, h], gr.at[l, h], "dp", mate)
-        readout = jnp.concatenate(
-            [ro[l, h].reshape(2 * r, cols), rg[l, h].reshape(2 * r, cols)], axis=0
-        )
-        mixed = jnp.dot(readout, wo_v[l], preferred_element_type=jnp.float32)
-        for j in range(nt):
-            mx[l, h, j] = mixed[:, j * own : (j + 1) * own].astype(jnp.bfloat16)
+        return readout
+
+    def mix(l, i, readout):
+        for k in range(2):
+            if i == 0 and k == 1:
+                arrived(wo_v.at[l, 1], wo_r.at[l])
+            mixed = jnp.dot(readout, wo_v[l, k], preferred_element_type=jnp.float32)
+            for j in range(nt):
+                mx[l, i, j, k] = mixed[:, j * own : (j + 1) * own].astype(jnp.bfloat16)
         for k, peer in tp_peers:
-            send(mx.at[l, h, peer], ms.at[l, h, k - 1], 4, ms_r.at[l, h], "tp", peer)
-
-    def collect(l, h):
-        total = mx[l, h, t].astype(jnp.float32)
-        total = total + xg[l, t, :, cut(h), :].reshape(nd * r, own).astype(jnp.float32)
-        arrived(ms.at[l, h], ms_r.at[l, h], "tp", tp_peers[0][1])
-        for k in range(nt - 1):
-            total = total + ms[l, h, k].astype(jnp.float32)
-        result = total.astype(jnp.bfloat16).reshape(nd, r, own)
-        if l + 1 < layers:
-            xg[l + 1, t, :, cut(h), :] = result
-            send_features(l + 1, h)
+            if l < last:
+                send(mx.at[l, i, peer], ms.at[l, i, k - 1], "ms", ms_r.at[l, i], {"tp": peer})
+            else:
+                send(mx.at[l, i, peer, 0], fo.at[i, k - 1], "fo", f_r.at[0, i], {"tp": peer})
+                send(
+                    mx.at[l, i, peer, 1],
+                    fm.at[i, k],
+                    "fm",
+                    f_r.at[1, i],
+                    {"tp": peer, "dp": mate},
+                )
+        if l == last:
+            send(mx.at[l, i, t, 1], fm.at[i, 0], "fm", f_r.at[1, i], {"dp": mate})
+        send(state_o.at[l, i, mate], state_m.at[l, i], "state", st_r.at[0], {"dp": mate})
+        send(branch_o.at[l, i, mate], branch_m.at[l, i], "branch", br_r.at[0], {"dp": mate})
+
+    def collect(l, i):
+        arrived(ms.at[l, i], ms_r.at[l, i])
+        for k in range(2):
+            total = mx[l, i, t, k].astype(jnp.float32)
+            total = total + xg[l, i, t, k].reshape(full, own).astype(jnp.float32)
+            for j in range(nt - 1):
+                total = total + ms[l, i, j, k].astype(jnp.float32)
+            xg[l + 1, i, t, k] = total.astype(jnp.bfloat16).reshape(nd, r, own)
+        block = xg.at[l + 1, i, t]
+        for _, peer in tp_peers:
+            send(block, block, "xg", xr.at[l + 1, i], {"tp": peer})
+        if l + 1 == last:
+            send(block.at[1], res.at[i], "res", res_r.at[i], {"dp": mate})
+
+    def finish(k, i):
+        if k == 0:
+            total = mx[last, i, t, 0].astype(jnp.float32)
+            total = total + xg[last, i, t, 0].reshape(full, own).astype(jnp.float32)
+            held = fo
         else:
-            mix_o[:, cut(h), :] = result
-
-    loaded(xg.at[0, t], c_stream)
-    pl.semaphore_wait(barrier, nt - 1 + 2)
-    for h in range(halves):
-        send_features(0, h)
+            arrived(res.at[i], res_r.at[i])
+            total = res[i].reshape(full, own).astype(jnp.float32)
+            held = fm
+        arrived(held.at[i], f_r.at[k, i])
+        for j in range(held.shape[1]):
+            total = total + held[i, j].astype(jnp.float32)
+        mix_o[k, i] = total.astype(jnp.bfloat16).reshape(nd, r, own)
+
+    for i in range(groups):
+        loaded(xg.at[0, i, t, 0], c_own[i])
+    loaded(xm, c_mate)
+    pl.semaphore_wait(barrier, 2 * (nt - 1) + 3)
+    for i in range(groups):
+        block = xg.at[0, i, t, 0]
+        for _, peer in tp_peers:
+            send(block, block, "xo", xr.at[0, i], {"tp": peer})
+            send(xm.at[i], xg.at[0, i, t, 1], "xm", xr_m.at[i], {"tp": peer, "dp": mate})
+        send(xm.at[i], xg.at[0, i, t, 1], "xm", xr_m.at[i], {"dp": mate})
+    loaded(gain_v.at[0], c_gain)
+    send(gain_v.at[0], gain_v.at[1], "gain", gain_r.at[0], {"dp": mate})
+    send_weights(0)
     for ref, sem in c_first:
         loaded(ref, sem)
     prepare()
     send_history(0)
+    send_out(0)
     for l in range(layers):
-        for h in range(halves):
-            project(l, h)
-            if h > 0:
-                halve(l, h - 1)
-        halve(l, halves - 1)
-        for h in range(halves):
-            recur(l, h)
-            if h > 0:
-                mix(l, h - 1)
-        mix(l, halves - 1)
+        for i in range(groups):
+            project(l, i)
+        if l + 1 < layers:
+            send_weights(l + 1)
+        for i in range(groups):
+            readout = recur(l, i)
+            mix(l, i, readout)
         if l + 1 < layers:
             send_history(l + 1)
-        for h in range(halves):
-            collect(l, h)
-    all_sent(xg.at[:, pl.ds(0, nt - 1)], 0, "tp", tp_peers[0][1])
-    all_sent(pr, 1, "dp", mate)
-    all_sent(px, 2, "dp", across)
-    all_sent(rg, 3, "dp", mate)
-    all_sent(ms, 4, "tp", tp_peers[0][1])
-    all_sent(aux.at[:, 0], 5, "dp", across)
+            send_out(l + 1)
+            for i in range(groups):
+                collect(l, i)
+    for i in range(groups):
+        finish(0, i)
+        finish(1, i)
+    arrived(state_m, st_r.at[0])
+    arrived(branch_m, br_r.at[0])
+    all_sent("xo", xg.at[0, :, pl.ds(0, nt - 1), 0])
+    all_sent("xm", xg.at[0, :, :, 1])
+    all_sent("gain", gain_v.at[1])
+    all_sent("wp", wp_v.at[:, 1])
+    all_sent("wo", wo_v.at[:, 1])
+    all_sent("aux", aux.at[:, pl.ds(0, nd - 1)])
+    all_sent("px", px)
+    all_sent("ms", ms)
+    all_sent("xg", xg.at[pl.ds(1, last), :, pl.ds(0, nt - 1)])
+    all_sent("res", res)
+    all_sent("fo", fo)
+    all_sent("fm", fm)
+    all_sent("state", state_m)
+    all_sent("branch", branch_m)
 
 
 def flipped(index, mask, count):
@@ -488,20 +561,29 @@
     return index
 
 
-def block_of(d, s):
+def tail_kernel(
+    mixed, state, state_m, hist, branch, branch_m, mixed_out, state_out, window_out, sem
+):
+    d = lax.axis_index("dp")
     core = lax.rem(d, 2)
-    return 2 * (s % 2) + (core if s < 2 else 1 - core)
-
-
-def tail_kernel(mixed, state, hist, branch, mixed_out, state_out, window_out, sem):
-    d = lax.axis_index("dp")
-    side = d // 2
     layers, depth = window_out.shape[:2]
-    pairs = [(mixed.at[s], mixed_out.at[block_of(d, s)]) for s in range(mixed.shape[0])]
+    groups, r = mixed.shape[1], mixed.shape[3]
+
+    def span(k, i):
+        side = core if k == 0 else 1 - core
+        return pl.ds(pl.multiple_of((side * groups + i) * r, r), r)
+
+    pairs = []
+    for i in range(groups):
+        for k in range(2):
+            pairs.append((mixed.at[k, i], mixed_out.at[:, span(k, i), :]))
     for l in range(layers):
-        pairs.append((state.at[l, side], state_out.at[l]))
         pairs.append((hist.at[l], window_out.at[l, pl.ds(0, depth - 1)]))
-        pairs.append((branch.at[l, side], window_out.at[l, depth - 1]))
+        for i in range(groups):
+            pairs.append((state.at[l, i, d], state_out.at[l, span(0, i), :]))
+            pairs.append((state_m.at[l, i], state_out.at[l, span(1, i), :]))
+            pairs.append((branch.at[l, i, d], window_out.at[l, depth - 1, span(0, i), :]))
+            pairs.append((branch_m.at[l, i], window_out.at[l, depth - 1, span(1, i), :]))
     stores = [pltpu.make_async_copy(src, dst, sem.at[k]) for k, (src, dst) in enumerate(pairs)]
     for copy in stores:
         copy.start()
@@ -512,7 +594,7 @@
 def fused(
     nt,
     nd,
-    halves,
+    groups,
     stream,
     lengths,
     prior_state,
@@ -529,7 +611,8 @@
     layers, width, cols = w_branch.shape
     batch, own = stream.shape
     rows = batch // nd
-    r = rows // halves
+    r = rows // (2 * groups)
+    full = nd * r
     depth = prior_window.shape[2]
     window = prior_window.transpose(0, 2, 1, 3)
     bf16, f32 = jnp.bfloat16, jnp.float32
@@ -537,43 +620,52 @@
     held = pl.BlockSpec(memory_space=pltpu.VMEM)
     dma = pltpu.SemaphoreType.DMA
     finals = pl.pallas_call(
-        functools.partial(fused_kernel, nt, nd, halves),
+        functools.partial(fused_kernel, nt, nd, groups),
         out_shape=(
-            pltpu.VMEM((nd, rows, own), bf16),
-            pltpu.VMEM((layers, 2, rows, cols), f32),
+            pltpu.VMEM((2, groups, nd, r, own), bf16),
+            pltpu.VMEM((layers, groups, nd, r, cols), f32),
+            pltpu.VMEM((layers, groups, r, cols), f32),
             pltpu.VMEM((layers, depth - 1, rows, cols), bf16),
-            pltpu.VMEM((layers, 2, rows, cols), bf16),
+            pltpu.VMEM((layers, groups, nd, r, cols), bf16),
+            pltpu.VMEM((layers, groups, r, cols), bf16),
         ),
         in_specs=[pl.BlockSpec(memory_space=pltpu.HBM)] * 12,
-        out_specs=(held,) * 4,
+        out_specs=(held,) * 6,
         scratch_shapes=[
-            pltpu.VMEM((layers, nt, nd, rows, own), bf16),
-            pltpu.VMEM((layers, halves, nd, r, 2 * cols + 128), bf16),
-            pltpu.VMEM((layers, halves, 2, r, 2 * cols + 128), bf16),
-            pltpu.VMEM((layers, halves, 2, r, 2 * cols + 128), bf16),
-            pltpu.VMEM((layers, halves, 2, r, 2 * cols + 128), bf16),
-            pltpu.VMEM((layers, halves, 2, r, cols), bf16),
-            pltpu.VMEM((layers, halves, 2, r, cols), bf16),
-            pltpu.VMEM((layers, halves, nt, nd * r, own), bf16),
-            pltpu.VMEM((layers, halves, nt - 1, nd * r, own), bf16),
-            pltpu.VMEM((layers, 2, 2, rows, cols), f32),
+            pltpu.VMEM((layers, groups, nt, 2, nd, r, own), bf16),
+            pltpu.VMEM((groups, nd, r, own), bf16),
+            pltpu.VMEM((layers, groups, full, 2 * cols + 128), bf16),
+            pltpu.VMEM((layers, groups, full, 2 * cols + 128), bf16),
+            pltpu.VMEM((layers, groups, nt, 2, full, own), bf16),
+            pltpu.VMEM((layers - 1, groups, nt - 1, 2, full, own), bf16),
+            pltpu.VMEM((groups, nt - 1, full, own), bf16),
+            pltpu.VMEM((groups, nt, full, own), bf16),
+            pltpu.VMEM((groups, nd, r, own), bf16),
+            pltpu.VMEM((layers, 2, groups, 2, r, cols), f32),
+            pltpu.VMEM((layers, nd, groups, 2, r, cols), f32),
             pltpu.VMEM((1, rows), jnp.int32),
             pltpu.VMEM(prior_state.shape, f32),
             pltpu.VMEM(window.shape, bf16),
-            pltpu.VMEM(norm_gain.shape, f32),
-            pltpu.VMEM((layers, 2, width, cols), bf16),
+            pltpu.VMEM((2,) + norm_gain.shape, f32),
+            pltpu.VMEM((layers, 2, 2, width, cols), bf16),
             pltpu.VMEM(conv_taps.shape, bf16),
             pltpu.VMEM((2, layers, BLOCK, cols), bf16),
             pltpu.VMEM(decay_param.shape, f32),
-            pltpu.VMEM(w_out.shape, bf16),
-            dma((8 + 2 * layers,)),
-            dma((6,)),
-            dma((layers, halves)),
-            dma((layers, halves)),
-            dma((layers, halves)),
-            dma((layers, halves)),
-            dma((layers, halves)),
+            pltpu.VMEM((layers, 2, cols, width), bf16),
+            dma((8 + groups + 2 * layers,)),
+            dma((14,)),
+            dma((layers, groups)),
+            dma((groups,)),
+            dma((layers, groups)),
+            dma((layers - 1, groups)),
+            dma((2, groups)),
+            dma((groups,)),
             dma((layers,)),
+            dma((layers,)),
+            dma((layers,)),
+            dma((1,)),
+            dma((1,)),
+            dma((1,)),
         ],
         compiler_params=pltpu.CompilerParams(
             collective_id=0, has_side_effects=True, vmem_limit_bytes=MAIN_VMEM
@@ -599,9 +691,9 @@
             jax.ShapeDtypeStruct(prior_state.shape, f32),
             jax.ShapeDtypeStruct(window.shape, bf16),
         ),
-        in_specs=[held] * 4,
+        in_specs=[held] * 6,
         out_specs=(anywhere,) * 3,
-        scratch_shapes=[dma((nd + 3 * layers,))],
+        scratch_shapes=[dma((2 * groups + layers * (1 + 4 * groups),))],
         compiler_params=pltpu.CompilerParams(vmem_limit_bytes=TAIL_VMEM),
     )(*finals)
     return mixed.reshape(batch, own), state, new_window.transpose(0, 2, 1, 3)
@@ -610,8 +702,9 @@
 def step(nt, nd, *arrays):
     stream, w_branch = arrays[0], arrays[5]
     rows, cols = stream.shape[0] // nd, w_branch.shape[2]
-    if nd == 4 and nt & (nt - 1) == 0 and cols % BLOCK == 0 and stream.shape[1] % 128 == 0 and rows % (8 * HALVES) == 0:
-        return fused(nt, nd, HALVES, *arrays)
+    layers = w_branch.shape[0]
+    if nd == 4 and layers > 1 and nt & (nt - 1) == 0 and cols % BLOCK == 0 and stream.shape[1] % 128 == 0 and rows % (16 * GROUPS) == 0:
+        return fused(nt, nd, GROUPS, *arrays)
     return body(*arrays)
 
 

time: 44.5 us -> 41.9 us (0.942)
  Pallas kernels: 43.6 us -> 41.1 us
    pallas_call x1, Pallas kernels: 42.8 us -> 40.2 us  [fused(): pl.pallas_call(functools.partial(fused_kernel, nt, nd, groups), out_shape...]
where the time goes in v2:
time: 41.9 us; the launch traced here: 41.8 us
  Pallas kernels  41.1 us (98%)
  between operations  0.64 us (2%)
    pallas_call x1, Pallas kernels, fused(): pl.pallas_call(functools.partial(fused_kernel, nt, nd, groups), out_shape...  40.2 us
    pallas_call x1, Pallas kernels, fused(): pl.pallas_call(tail_kernel, out_shape=(jax.ShapeDtypeStruct((nd, rows, ow...  0.93 us

profile of v2, /device:TPU:0, one launch (start us, length us, event | category | flops | bytes accessed | tf_op | source)
XLA Modules:
  0.0 41.8 jit_solution(4806789433158859760)
XLA Ops:
  0.6 40.2 %shard_map.139 = (bf16[2,2,4,8,128]{4,3,2,1,0:T(8,128)(2,1)S(1)}, f32[2,2,4,8,512]{4,3,2,1,0:T(8,128)S(1)}, f32[2,2,8,512]{3,2,1,0:T(8,128)S(1)}, bf16[2,2,32,51...) custom-call(bf16[4,32,128]{2,1,0:T(8,128)(2,1)} %bitcast.6, ...), custom_call_target="tpu_custom_call" | custom-call | tf_op jit(solution)/shard_map/pallas_call | solution.py:622
  40.8 0.9 %shard_map.140 = (bf16[4,32,128]{2,1,0:T(8,128)(2,1)}, f32[2,32,512]{2,1,0:T(8,128)}, bf16[2,3,32,512]{3,2,1,0:T(8,128)(2,1)}) custom-call(bf16[2,2,4,8,128]{4,3,2,1,0:T(8,128)(2,1)S(1)} %get-tuple-element.12.mixed, f32[2,2,4,8,512]{4,3,2,1,0:T(8,128)S(1)} %get-tuple-element.13.state, f32[2,2,8,512]{3,2,1,0:T(8,128)S(1)} %get-tuple-element.14.state_m, ...), custom_call_target="tpu_custom_call" | custom-call | tf_op jit(solution)/shard_map/pallas_call | solution.py:687

commit v3 on v2

--- a/solution.py
+++ b/solution.py
@@ -223,6 +223,9 @@
     fo,
     fm,
     res,
+    mq,
+    rq,
+    xq,
     am,
     aux,
     len_v,
@@ -234,14 +237,18 @@
     gates_v,
     decay_v,
     wo_v,
+    gain_s,
+    acc,
+    sq,
     in_sem,
     sent,
     xr,
-    xr_m,
     px_r,
     ms_r,
     f_r,
     res_r,
+    mq_r,
+    rq_r,
     aux_r,
     wp_r,
     wo_r,
@@ -263,6 +270,8 @@
     cols = w_branch.shape[2]
     width = w_branch.shape[1]
     depth = prior_window.shape[1]
+
+    halves_of = (pl.ds(0, 128 + cols), pl.ds(128 + cols, cols))
 
     barrier = pltpu.get_barrier_semaphore()
     tp_peers = [(k, flipped(t, k, nt)) for k in range(nt - 1, 0, -1)]
@@ -374,36 +383,79 @@
         loaded(wo_v.at[l, 0], c_o[l])
         send(wo_v.at[l, 0], wo_v.at[l, 1], "wo", wo_r.at[l], {"dp": mate})
 
-    def project(l, i):
+    def spread_gain(k):
+        for l in range(layers):
+            for j in range(nt):
+                gain_s[k, l, j] = gain_v[k, l : l + 1, j * own : (j + 1) * own]
+
+    def normed(l, i, k, first):
+        squares = jnp.zeros((full, own), jnp.float32)
+        pieces = []
+        for j in range(nt // 2):
+            x = xg[l, i, first + j, k].reshape(full, own).astype(jnp.float32)
+            squares = squares + x * x
+            pieces.append((x * gain_s[k, l, first + j]).astype(jnp.bfloat16))
+        return jnp.concatenate(pieces, axis=1), squares
+
+    def weight(l, k, w, first):
+        return wp_v[l, k, w, pl.ds(pl.multiple_of(first * own, own * nt // 2), own * nt // 2), :]
+
+    def project_near(l, i):
         if l == 0:
-            arrived(xg.at[l, i, pl.ds(0, nt - 1), 0], xr.at[l, i])
-            arrived(xg.at[l, i, :, 1], xr_m.at[i])
+            arrived(xg.at[l, i, pl.ds(0, nt - 1), 0], xr.at[l, i, 0])
         else:
-            arrived(xg.at[l, i, pl.ds(0, nt - 1)], xr.at[l, i])
+
+            @pl.when(core == 1)
+            def _():
+                arrived(xg.at[l, i, pl.ds(0, nt // 2 - 1)], xr.at[l, i, 0])
+
+            @pl.when(core == 0)
+            def _():
+                arrived(xg.at[l, i, pl.ds(0, nt // 2)], xr.at[l, i, 0])
+
+        if l < last:
+
+            @pl.when(core == 0)
+            def _():
+                send(xg.at[l, i, t], rq.at[l, i], "rq", rq_r.at[l, i], {"dp": mate})
+
+        first = t // (nt // 2) * (nt // 2)
         if i == 0 and l == 0:
             arrived(gain_v.at[1], gain_r.at[0])
-        squares = jnp.zeros((full, own), jnp.float32)
+            spread_gain(1)
+        squares = []
         products = [None, None]
         for k in range(2):
-            pieces = []
-            for j in range(nt):
-                x = xg[l, i, j, k].reshape(full, own).astype(jnp.float32)
-                squares = squares + x * x
-                gain = gain_v[k, l : l + 1, j * own : (j + 1) * own]
-                pieces.append((x * gain).astype(jnp.bfloat16))
-            normed = jnp.concatenate(pieces, axis=1)
+            x, part_squares = normed(l, i, k, first)
+            squares.append(part_squares)
             if i == 0 and k == 1:
                 arrived(wp_v.at[l, 1], wp_r.at[l])
             for w in range(2):
-                term = jnp.dot(normed, wp_v[l, k, w], preferred_element_type=jnp.float32)
+                term = jnp.dot(x, weight(l, k, w, first), preferred_element_type=jnp.float32)
                 products[w] = term if k == 0 else products[w] + term
-        total = jnp.sum(squares, axis=1, keepdims=True)
+        for w in range(2):
+            acc[i, w] = products[w]
+        sq[i] = squares[0] + squares[1]
+
+    def project_far(l, i):
+        arrived(xg.at[l, i, pl.ds(0, nt // 2)], xr.at[l, i, 1])
+        first = (1 - t // (nt // 2)) * (nt // 2)
+        x0, squares0 = normed(l, i, 0, first)
+        x1, squares1 = normed(l, i, 1, first)
+        total = jnp.sum(sq[i] + squares0 + squares1, axis=1, keepdims=True)
         high = total.astype(jnp.bfloat16).astype(jnp.float32)
         lane = lax.broadcasted_iota(jnp.int32, (full, 128), 1)
-        part[l, i, :, 2 * cols :] = jnp.where(lane < 64, high, total - high).astype(jnp.bfloat16)
+        part[l, i, :, :128] = jnp.where(lane < 64, high, total - high).astype(jnp.bfloat16)
         for w in range(2):
-            part[l, i, :, w * cols : (w + 1) * cols] = products[w].astype(jnp.bfloat16)
-        send(part.at[l, i], px.at[l, i], "px", px_r.at[l, i], {"dp": across})
+            product = acc[i, w] + jnp.dot(
+                x0, weight(l, 0, w, first), preferred_element_type=jnp.float32
+            )
+            product = product + jnp.dot(
+                x1, weight(l, 1, w, first), preferred_element_type=jnp.float32
+            )
+            part[l, i, :, 128 + w * cols : 128 + (w + 1) * cols] = product.astype(jnp.bfloat16)
+            ready = halves_of[w]
+            send(part.at[l, i, :, ready], px.at[l, i, :, ready], "px", px_r.at[l, i, w], {"dp": across})
 
     def recur(l, i):
         if i == 0:
@@ -416,12 +468,12 @@
         taps = taps_v[l].astype(jnp.float32)
         raw = decay_v[l : l + 1]
         log_decay = jnp.minimum(raw, 0.0) - jnp.log1p(jnp.exp(-jnp.abs(raw)))
-        arrived(px.at[l, i], px_r.at[l, i])
-        summed = part[l, i].astype(jnp.float32) + px[l, i].astype(jnp.float32)
-        squares = summed[:, 2 * cols : 2 * cols + 1] + summed[:, 2 * cols + 64 : 2 * cols + 65]
+        first, second = halves_of
+        arrived(px.at[l, i, :, first], px_r.at[l, i, 0])
+        summed = part[l, i, :, first].astype(jnp.float32) + px[l, i, :, first].astype(jnp.float32)
+        squares = summed[:, :1] + summed[:, 64:65]
         scaling = lax.rsqrt(squares / (width * nd) + epsilon)
-        branch = (summed[:, :cols] * scaling).astype(jnp.bfloat16)
-        gate_in = (summed[:, cols : 2 * cols] * scaling).astype(jnp.bfloat16)
+        branch = (summed[:, 128:] * scaling).astype(jnp.bfloat16)
         branch_o[l, i] = branch.reshape(nd, r, cols)
         convolved = (before + branch.astype(jnp.float32) * taps[depth : depth + 1]).astype(
             jnp.bfloat16
@@ -447,6 +499,9 @@
         feeding = jnp.sqrt(negative_expm1(2.0 * log_keep))
         state = jnp.exp(log_keep) * earlier + feeding * input_gate * convolved.astype(jnp.float32)
         state_o[l, i] = state.reshape(nd, r, cols)
+        arrived(px.at[l, i, :, second], px_r.at[l, i, 1])
+        summed = part[l, i, :, second].astype(jnp.float32) + px[l, i, :, second].astype(jnp.float32)
+        gate_in = (summed * scaling).astype(jnp.bfloat16)
         readout = (state * jax.nn.gelu(gate_in.astype(jnp.float32))).astype(jnp.bfloat16)
         return readout
 
@@ -457,20 +512,31 @@
             mixed = jnp.dot(readout, wo_v[l, k], preferred_element_type=jnp.float32)
             for j in range(nt):
                 mx[l, i, j, k] = mixed[:, j * own : (j + 1) * own].astype(jnp.bfloat16)
-        for k, peer in tp_peers:
             if l < last:
-                send(mx.at[l, i, peer], ms.at[l, i, k - 1], "ms", ms_r.at[l, i], {"tp": peer})
-            else:
-                send(mx.at[l, i, peer, 0], fo.at[i, k - 1], "fo", f_r.at[0, i], {"tp": peer})
-                send(
-                    mx.at[l, i, peer, 1],
-                    fm.at[i, k],
-                    "fm",
-                    f_r.at[1, i],
-                    {"tp": peer, "dp": mate},
-                )
-        if l == last:
-            send(mx.at[l, i, t, 1], fm.at[i, 0], "fm", f_r.at[1, i], {"dp": mate})
+
+                @pl.when(core == 1)
+                def _():
+                    for n, peer in tp_peers:
+                        block = mx.at[l, i, peer, k]
+                        send(block, ms.at[l, i, n - 1, k], "ms", ms_r.at[l, i], {"tp": peer})
+
+                @pl.when(core == 0)
+                def _():
+                    for n, peer in tp_peers:
+                        block, where = mx.at[l, i, peer, k], {"tp": peer, "dp": mate}
+                        send(block, mq.at[l, i, n, k], "mq", mq_r.at[l, i], where)
+                    block = mx.at[l, i, t, k]
+                    send(block, mq.at[l, i, 0, k], "mq", mq_r.at[l, i], {"dp": mate})
+
+                continue
+            for n, peer in tp_peers:
+                block = mx.at[l, i, peer, k]
+                if k == 0:
+                    send(block, fo.at[i, n - 1], "fo", f_r.at[0, i], {"tp": peer})
+                else:
+                    send(block, fm.at[i, n], "fm", f_r.at[1, i], {"tp": peer, "dp": mate})
+            if l == last and k == 1:
+                send(mx.at[l, i, t, 1], fm.at[i, 0], "fm", f_r.at[1, i], {"dp": mate})
         send(state_o.at[l, i, mate], state_m.at[l, i], "state", st_r.at[0], {"dp": mate})
         send(branch_o.at[l, i, mate], branch_m.at[l, i], "branch", br_r.at[0], {"dp": mate})
 
@@ -483,10 +549,23 @@
                 total = total + ms[l, i, j, k].astype(jnp.float32)
             xg[l + 1, i, t, k] = total.astype(jnp.bfloat16).reshape(nd, r, own)
         block = xg.at[l + 1, i, t]
-        for _, peer in tp_peers:
-            send(block, block, "xg", xr.at[l + 1, i], {"tp": peer})
+        for n, peer in tp_peers:
+            send(block, block, "xg", xr.at[l + 1, i, 2 * n // nt], {"tp": peer})
         if l + 1 == last:
             send(block.at[1], res.at[i], "res", res_r.at[i], {"dp": mate})
+
+    def collect_mate(l, i):
+        arrived(rq.at[l, i], rq_r.at[l, i])
+        arrived(mq.at[l, i], mq_r.at[l, i])
+        for k in range(2):
+            total = rq[l, i, k].reshape(full, own).astype(jnp.float32)
+            for j in range(nt):
+                total = total + mq[l, i, j, k].astype(jnp.float32)
+            xq[l, i, k] = total.astype(jnp.bfloat16).reshape(nd, r, own)
+        block, dst = xq.at[l, i], xg.at[l + 1, i, t]
+        for n, peer in tp_peers:
+            send(block, dst, "xq", xr.at[l + 1, i, 2 * n // nt], {"tp": peer, "dp": mate})
+        send(block, dst, "xq", xr.at[l + 1, i, 0], {"dp": mate})
 
     def finish(k, i):
         if k == 0:
@@ -494,7 +573,16 @@
             total = total + xg[last, i, t, 0].reshape(full, own).astype(jnp.float32)
             held = fo
         else:
-            arrived(res.at[i], res_r.at[i])
+
+
+            @pl.when(core == 0)
+            def _():
+                arrived(res.at[i], res_r.at[i])
+
+            @pl.when(core == 1)
+            def _():
+                res[i] = xq[last - 1, i, 1]
+
             total = res[i].reshape(full, own).astype(jnp.float32)
             held = fm
         arrived(held.at[i], f_r.at[k, i])
@@ -506,23 +594,42 @@
         loaded(xg.at[0, i, t, 0], c_own[i])
     loaded(xm, c_mate)
     pl.semaphore_wait(barrier, 2 * (nt - 1) + 3)
-    for i in range(groups):
+    def send_own(i):
         block = xg.at[0, i, t, 0]
-        for _, peer in tp_peers:
-            send(block, block, "xo", xr.at[0, i], {"tp": peer})
-            send(xm.at[i], xg.at[0, i, t, 1], "xm", xr_m.at[i], {"tp": peer, "dp": mate})
-        send(xm.at[i], xg.at[0, i, t, 1], "xm", xr_m.at[i], {"dp": mate})
+        for n, peer in tp_peers:
+            send(block, block, "xo", xr.at[0, i, 2 * n // nt], {"tp": peer})
+
+    def send_mate(i):
+        for n, peer in tp_peers:
+            sem = xr.at[0, i, 2 * n // nt]
+            send(xm.at[i], xg.at[0, i, t, 1], "xm", sem, {"tp": peer, "dp": mate})
+        send(xm.at[i], xg.at[0, i, t, 1], "xm", xr.at[0, i, 0], {"dp": mate})
+
+    for kind, calls in enumerate(((send_own, send_mate), (send_mate, send_own))):
+
+        @pl.when(core == kind)
+        def _():
+            for i in range(groups):
+                for call in calls:
+                    call(i)
+
     loaded(gain_v.at[0], c_gain)
     send(gain_v.at[0], gain_v.at[1], "gain", gain_r.at[0], {"dp": mate})
     send_weights(0)
     for ref, sem in c_first:
         loaded(ref, sem)
+    spread_gain(0)
     prepare()
     send_history(0)
     send_out(0)
     for l in range(layers):
+        if l == 0:
+            for i in range(groups):
+                project_near(l, i)
         for i in range(groups):
-            project(l, i)
+            if l > 0:
+                project_near(l, i)
+            project_far(l, i)
         if l + 1 < layers:
             send_weights(l + 1)
         for i in range(groups):
@@ -531,8 +638,14 @@
         if l + 1 < layers:
             send_history(l + 1)
             send_out(l + 1)
-            for i in range(groups):
-                collect(l, i)
+
+
+            @pl.when(core == 1)
+            def _():
+                for i in range(groups):
+                    collect(l, i)
+                    collect_mate(l, i)
+
     for i in range(groups):
         finish(0, i)
         finish(1, i)
@@ -545,9 +658,19 @@
     all_sent("wo", wo_v.at[:, 1])
     all_sent("aux", aux.at[:, pl.ds(0, nd - 1)])
     all_sent("px", px)
-    all_sent("ms", ms)
-    all_sent("xg", xg.at[pl.ds(1, last), :, pl.ds(0, nt - 1)])
-    all_sent("res", res)
+
+    @pl.when(core == 1)
+    def _():
+        all_sent("ms", ms)
+        all_sent("xg", xg.at[pl.ds(1, last), :, pl.ds(0, nt - 1)])
+        all_sent("xq", xg.at[pl.ds(1, last)])
+        all_sent("res", res)
+
+    @pl.when(core == 0)
+    def _():
+        all_sent("mq", mq)
+        all_sent("rq", rq)
+
     all_sent("fo", fo)
     all_sent("fm", fm)
     all_sent("state", state_m)
@@ -641,6 +764,9 @@
             pltpu.VMEM((groups, nt - 1, full, own), bf16),
             pltpu.VMEM((groups, nt, full, own), bf16),
             pltpu.VMEM((groups, nd, r, own), bf16),
+            pltpu.VMEM((layers - 1, groups, nt, 2, full, own), bf16),
+            pltpu.VMEM((layers - 1, groups, 2, nd, r, own), bf16),
+            pltpu.VMEM((layers - 1, groups, 2, nd, r, own), bf16),
             pltpu.VMEM((layers, 2, groups, 2, r, cols), f32),
             pltpu.VMEM((layers, nd, groups, 2, r, cols), f32),
             pltpu.VMEM((1, rows), jnp.int32),
@@ -652,14 +778,18 @@
             pltpu.VMEM((2, layers, BLOCK, cols), bf16),
             pltpu.VMEM(decay_param.shape, f32),
             pltpu.VMEM((layers, 2, cols, width), bf16),
+            pltpu.VMEM((2, layers, nt, 1, own), f32),
+            pltpu.VMEM((groups, 2, full, cols), f32),
+            pltpu.VMEM((groups, full, own), f32),
             dma((8 + groups + 2 * layers,)),
-            dma((14,)),
-            dma((layers, groups)),
-            dma((groups,)),
-            dma((layers, groups)),
+            dma((17,)),
+            dma((layers, groups, 2)),
+            dma((layers, groups, 2)),
             dma((layers - 1, groups)),
             dma((2, groups)),
             dma((groups,)),
+            dma((layers - 1, groups)),
+            dma((layers - 1, groups)),
             dma((layers,)),
             dma((layers,)),
             dma((layers,)),

time: 41.9 us -> 40.3 us (0.962)
  Pallas kernels: 41.1 us -> 39.5 us
    pallas_call x1, Pallas kernels: 40.2 us -> 38.6 us  [fused(): pl.pallas_call(functools.partial(fused_kernel, nt, nd, groups), out_shape...]
where the time goes in v3:
time: 40.3 us; the launch traced here: 40.1 us
  Pallas kernels  39.5 us (98%)
  between operations  0.64 us (2%)
    pallas_call x1, Pallas kernels, fused(): pl.pallas_call(functools.partial(fused_kernel, nt, nd, groups), out_shape...  38.6 us
    pallas_call x1, Pallas kernels, fused(): pl.pallas_call(tail_kernel, out_shape=(jax.ShapeDtypeStruct((nd, rows, ow...  0.93 us

profile of v3, /device:TPU:0, one launch (start us, length us, event | category | flops | bytes accessed | tf_op | source)
XLA Modules:
  0.0 40.1 jit_solution(11863097862590415949)
XLA Ops:
  0.6 38.6 %shard_map.139 = (bf16[2,2,4,8,128]{4,3,2,1,0:T(8,128)(2,1)S(1)}, f32[2,2,4,8,512]{4,3,2,1,0:T(8,128)S(1)}, f32[2,2,8,512]{3,2,1,0:T(8,128)S(1)}, bf16[2,2,32,51...) custom-call(bf16[4,32,128]{2,1,0:T(8,128)(2,1)} %bitcast.6, ...), custom_call_target="tpu_custom_call" | custom-call | tf_op jit(solution)/shard_map/pallas_call | solution.py:745
  39.2 0.9 %shard_map.140 = (bf16[4,32,128]{2,1,0:T(8,128)(2,1)}, f32[2,32,512]{2,1,0:T(8,128)}, bf16[2,3,32,512]{3,2,1,0:T(8,128)(2,1)}) custom-call(bf16[2,2,4,8,128]{4,3,2,1,0:T(8,128)(2,1)S(1)} %get-tuple-element.12.mixed, f32[2,2,4,8,512]{4,3,2,1,0:T(8,128)S(1)} %get-tuple-element.13.state, f32[2,2,8,512]{3,2,1,0:T(8,128)S(1)} %get-tuple-element.14.state_m, ...), custom_call_target="tpu_custom_call" | custom-call | tf_op jit(solution)/shard_map/pallas_call | solution.py:817

commit v4 on v3

--- a/solution.py
+++ b/solution.py
@@ -226,6 +226,8 @@
     mq,
     rq,
     xq,
+    zs,
+    zr,
     am,
     aux,
     len_v,
@@ -249,6 +251,7 @@
     res_r,
     mq_r,
     rq_r,
+    z_r,
     aux_r,
     wp_r,
     wo_r,
@@ -271,10 +274,14 @@
     width = w_branch.shape[1]
     depth = prior_window.shape[1]
 
+    half = nt // 2
+    place = lax.rem(t, half)
     halves_of = (pl.ds(0, 128 + cols), pl.ds(128 + cols, cols))
 
     barrier = pltpu.get_barrier_semaphore()
     tp_peers = [(k, flipped(t, k, nt)) for k in range(nt - 1, 0, -1)]
+    opposite = flipped(t, half, nt)
+    tp_near = [(k, peer) for k, peer in tp_peers if k < half]
     for _, peer in tp_peers:
         for other in (d, mate):
             pl.semaphore_signal(
@@ -388,10 +395,10 @@
             for j in range(nt):
                 gain_s[k, l, j] = gain_v[k, l : l + 1, j * own : (j + 1) * own]
 
-    def normed(l, i, k, first):
+    def normed(l, i, k, first, count=nt // 2):
         squares = jnp.zeros((full, own), jnp.float32)
         pieces = []
-        for j in range(nt // 2):
+        for j in range(count):
             x = xg[l, i, first + j, k].reshape(full, own).astype(jnp.float32)
             squares = squares + x * x
             pieces.append((x * gain_s[k, l, first + j]).astype(jnp.bfloat16))
@@ -401,26 +408,9 @@
         return wp_v[l, k, w, pl.ds(pl.multiple_of(first * own, own * nt // 2), own * nt // 2), :]
 
     def project_near(l, i):
-        if l == 0:
-            arrived(xg.at[l, i, pl.ds(0, nt - 1), 0], xr.at[l, i, 0])
-        else:
-
-            @pl.when(core == 1)
-            def _():
-                arrived(xg.at[l, i, pl.ds(0, nt // 2 - 1)], xr.at[l, i, 0])
-
-            @pl.when(core == 0)
-            def _():
-                arrived(xg.at[l, i, pl.ds(0, nt // 2)], xr.at[l, i, 0])
-
-        if l < last:
-
-            @pl.when(core == 0)
-            def _():
-                send(xg.at[l, i, t], rq.at[l, i], "rq", rq_r.at[l, i], {"dp": mate})
-
+        arrived(xg.at[l, i, pl.ds(0, nt - 1), 0], xr.at[l, i, 0])
         first = t // (nt // 2) * (nt // 2)
-        if i == 0 and l == 0:
+        if i == 0:
             arrived(gain_v.at[1], gain_r.at[0])
             spread_gain(1)
         squares = []
@@ -439,20 +429,49 @@
 
     def project_far(l, i):
         arrived(xg.at[l, i, pl.ds(0, nt // 2)], xr.at[l, i, 1])
+        send_before(l, i)
         first = (1 - t // (nt // 2)) * (nt // 2)
         x0, squares0 = normed(l, i, 0, first)
         x1, squares1 = normed(l, i, 1, first)
-        total = jnp.sum(sq[i] + squares0 + squares1, axis=1, keepdims=True)
+        publish(l, i, sq[i] + squares0 + squares1, x0, x1, first, nt // 2)
+
+    def project_all(l, i):
+        @pl.when(core == 1)
+        def _():
+            arrived(xg.at[l, i, pl.ds(0, 2 * half - 2)], xr.at[l, i, 0])
+
+        @pl.when(core == 0)
+        def _():
+            arrived(xg.at[l, i], xr.at[l, i, 0])
+
+        if l < last:
+            send_before(l, i)
+        x0, squares0 = normed(l, i, 0, 0, nt)
+        x1, squares1 = normed(l, i, 1, 0, nt)
+        if i == 0:
+            arrived(wp_v.at[l, 1], wp_r.at[l])
+        publish(l, i, squares0 + squares1, x0, x1, 0, nt)
+
+    def send_before(l, i):
+        @pl.when(core == 0)
+        def _():
+            for h in range(2):
+                block = xg.at[l, i, h * half + place]
+                send(block, rq.at[l, i, h], "rq", rq_r.at[l, i], {"dp": mate})
+
+    def publish(l, i, squares, x0, x1, first, count):
+        total = jnp.sum(squares, axis=1, keepdims=True)
         high = total.astype(jnp.bfloat16).astype(jnp.float32)
         lane = lax.broadcasted_iota(jnp.int32, (full, 128), 1)
         part[l, i, :, :128] = jnp.where(lane < 64, high, total - high).astype(jnp.bfloat16)
         for w in range(2):
-            product = acc[i, w] + jnp.dot(
-                x0, weight(l, 0, w, first), preferred_element_type=jnp.float32
-            )
-            product = product + jnp.dot(
-                x1, weight(l, 1, w, first), preferred_element_type=jnp.float32
-            )
+            product = None
+            for k, x in enumerate((x0, x1)):
+                table = wp_v[l, k, w] if count == nt else weight(l, k, w, first)
+                term = jnp.dot(x, table, preferred_element_type=jnp.float32)
+                product = term if product is None else product + term
+            if count < nt:
+                product = product + acc[i, w]
             part[l, i, :, 128 + w * cols : 128 + (w + 1) * cols] = product.astype(jnp.bfloat16)
             ready = halves_of[w]
             send(part.at[l, i, :, ready], px.at[l, i, :, ready], "px", px_r.at[l, i, w], {"dp": across})
@@ -513,21 +532,6 @@
             for j in range(nt):
                 mx[l, i, j, k] = mixed[:, j * own : (j + 1) * own].astype(jnp.bfloat16)
             if l < last:
-
-                @pl.when(core == 1)
-                def _():
-                    for n, peer in tp_peers:
-                        block = mx.at[l, i, peer, k]
-                        send(block, ms.at[l, i, n - 1, k], "ms", ms_r.at[l, i], {"tp": peer})
-
-                @pl.when(core == 0)
-                def _():
-                    for n, peer in tp_peers:
-                        block, where = mx.at[l, i, peer, k], {"tp": peer, "dp": mate}
-                        send(block, mq.at[l, i, n, k], "mq", mq_r.at[l, i], where)
-                    block = mx.at[l, i, t, k]
-                    send(block, mq.at[l, i, 0, k], "mq", mq_r.at[l, i], {"dp": mate})
-
                 continue
             for n, peer in tp_peers:
                 block = mx.at[l, i, peer, k]
@@ -537,35 +541,78 @@
                     send(block, fm.at[i, n], "fm", f_r.at[1, i], {"tp": peer, "dp": mate})
             if l == last and k == 1:
                 send(mx.at[l, i, t, 1], fm.at[i, 0], "fm", f_r.at[1, i], {"dp": mate})
+        if l < last:
+
+            @pl.when(core == 1)
+            def _():
+                for n, peer in tp_near:
+                    for h in range(2):
+                        block = mx.at[l, i, h * half + lax.rem(peer, half)]
+                        send(block, ms.at[l, i, n - 1, h], "ms", ms_r.at[l, i], {"tp": peer})
+
+            @pl.when(core == 0)
+            def _():
+                for n, peer in tp_near:
+                    for h in range(2):
+                        block = mx.at[l, i, h * half + lax.rem(peer, half)]
+                        where = {"tp": peer, "dp": mate}
+                        send(block, mq.at[l, i, n, h], "mq", mq_r.at[l, i], where)
+                for h in range(2):
+                    block = mx.at[l, i, h * half + place]
+                    send(block, mq.at[l, i, 0, h], "mq", mq_r.at[l, i], {"dp": mate})
+
         send(state_o.at[l, i, mate], state_m.at[l, i], "state", st_r.at[0], {"dp": mate})
         send(branch_o.at[l, i, mate], branch_m.at[l, i], "branch", br_r.at[0], {"dp": mate})
 
     def collect(l, i):
         arrived(ms.at[l, i], ms_r.at[l, i])
-        for k in range(2):
-            total = mx[l, i, t, k].astype(jnp.float32)
-            total = total + xg[l, i, t, k].reshape(full, own).astype(jnp.float32)
-            for j in range(nt - 1):
-                total = total + ms[l, i, j, k].astype(jnp.float32)
-            xg[l + 1, i, t, k] = total.astype(jnp.bfloat16).reshape(nd, r, own)
-        block = xg.at[l + 1, i, t]
-        for n, peer in tp_peers:
-            send(block, block, "xg", xr.at[l + 1, i, 2 * n // nt], {"tp": peer})
+        for h in range(2):
+            for k in range(2):
+                total = mx[l, i, h * half + place, k].astype(jnp.float32)
+                for j in range(half - 1):
+                    total = total + ms[l, i, j, h, k].astype(jnp.float32)
+                zs[l, 0, i, h, k] = total.astype(jnp.bfloat16)
+        send(zs.at[l, 0, i], zr.at[l, 0, i], "zs", z_r.at[l, 0, i], {"tp": opposite})
+
+    def collect_mate(l, i):
+        arrived(mq.at[l, i], mq_r.at[l, i])
+        for h in range(2):
+            for k in range(2):
+                total = mq[l, i, 0, h, k].astype(jnp.float32)
+                for j in range(1, half):
+                    total = total + mq[l, i, j, h, k].astype(jnp.float32)
+                zs[l, 1, i, h, k] = total.astype(jnp.bfloat16)
+        send(zs.at[l, 1, i], zr.at[l, 1, i], "zs", z_r.at[l, 1, i], {"tp": opposite})
+
+    def whole(l, which, i, h, k, before):
+        total = zs[l, which, i, h, k].astype(jnp.float32) + zr[l, which, i, h, k].astype(jnp.float32)
+        total = total + before.reshape(full, own).astype(jnp.float32)
+        return total.astype(jnp.bfloat16).reshape(nd, r, own)
+
+    def expand(l, i):
+        arrived(zr.at[l, 0, i], z_r.at[l, 0, i])
+        for h in range(2):
+            for k in range(2):
+                before = xg[l, i, h * half + place, k]
+                xg[l + 1, i, h * half + place, k] = whole(l, 0, i, h, k, before)
+        for _, peer in tp_near:
+            for h in range(2):
+                block = xg.at[l + 1, i, h * half + place]
+                send(block, block, "xg", xr.at[l + 1, i, 0], {"tp": peer})
         if l + 1 == last:
-            send(block.at[1], res.at[i], "res", res_r.at[i], {"dp": mate})
-
-    def collect_mate(l, i):
+            send(xg.at[l + 1, i, t, 1], res.at[i], "res", res_r.at[i], {"dp": mate})
+
+    def expand_mate(l, i):
         arrived(rq.at[l, i], rq_r.at[l, i])
-        arrived(mq.at[l, i], mq_r.at[l, i])
-        for k in range(2):
-            total = rq[l, i, k].reshape(full, own).astype(jnp.float32)
-            for j in range(nt):
-                total = total + mq[l, i, j, k].astype(jnp.float32)
-            xq[l, i, k] = total.astype(jnp.bfloat16).reshape(nd, r, own)
-        block, dst = xq.at[l, i], xg.at[l + 1, i, t]
-        for n, peer in tp_peers:
-            send(block, dst, "xq", xr.at[l + 1, i, 2 * n // nt], {"tp": peer, "dp": mate})
-        send(block, dst, "xq", xr.at[l + 1, i, 0], {"dp": mate})
+        arrived(zr.at[l, 1, i], z_r.at[l, 1, i])
+        for h in range(2):
+            for k in range(2):
+                xq[l, i, h, k] = whole(l, 1, i, h, k, rq[l, i, h, k])
+        for h in range(2):
+            block, dst = xq.at[l, i, h], xg.at[l + 1, i, h * half + place]
+            for _, peer in tp_near:
+                send(block, dst, "xq", xr.at[l + 1, i, 0], {"tp": peer, "dp": mate})
+            send(block, dst, "xq", xr.at[l + 1, i, 0], {"dp": mate})
 
     def finish(k, i):
         if k == 0:
@@ -581,7 +628,7 @@
 
             @pl.when(core == 1)
             def _():
-                res[i] = xq[last - 1, i, 1]
+                res[i] = xq[last - 1, i, t // half, 1]
 
             total = res[i].reshape(full, own).astype(jnp.float32)
             held = fm
@@ -628,8 +675,9 @@
                 project_near(l, i)
         for i in range(groups):
             if l > 0:
-                project_near(l, i)
-            project_far(l, i)
+                project_all(l, i)
+            else:
+                project_far(l, i)
         if l + 1 < layers:
             send_weights(l + 1)
         for i in range(groups):
@@ -642,9 +690,15 @@
 
             @pl.when(core == 1)
             def _():
-                for i in range(groups):
+                collect(l, 0)
+                collect_mate(l, 0)
+                for i in range(1, groups):
                     collect(l, i)
+                    expand(l, i - 1)
                     collect_mate(l, i)
+                    expand_mate(l, i - 1)
+                expand(l, groups - 1)
+                expand_mate(l, groups - 1)
 
     for i in range(groups):
         finish(0, i)
@@ -662,7 +716,8 @@
     @pl.when(core == 1)
     def _():
         all_sent("ms", ms)
-        all_sent("xg", xg.at[pl.ds(1, last), :, pl.ds(0, nt - 1)])
+        all_sent("zs", zr)
+        all_sent("xg", xg.at[pl.ds(1, last), :, pl.ds(0, 2 * half - 2)])
         all_sent("xq", xg.at[pl.ds(1, last)])
         all_sent("res", res)
 
@@ -760,13 +815,15 @@
             pltpu.VMEM((layers, groups, full, 2 * cols + 128), bf16),
             pltpu.VMEM((layers, groups, full, 2 * cols + 128), bf16),
             pltpu.VMEM((layers, groups, nt, 2, full, own), bf16),
-            pltpu.VMEM((layers - 1, groups, nt - 1, 2, full, own), bf16),
+            pltpu.VMEM((layers - 1, groups, nt // 2 - 1, 2, 2, full, own), bf16),
             pltpu.VMEM((groups, nt - 1, full, own), bf16),
             pltpu.VMEM((groups, nt, full, own), bf16),
             pltpu.VMEM((groups, nd, r, own), bf16),
-            pltpu.VMEM((layers - 1, groups, nt, 2, full, own), bf16),
-            pltpu.VMEM((layers - 1, groups, 2, nd, r, own), bf16),
-            pltpu.VMEM((layers - 1, groups, 2, nd, r, own), bf16),
+            pltpu.VMEM((layers - 1, groups, nt // 2, 2, 2, full, own), bf16),
+            pltpu.VMEM((layers - 1, groups, 2, 2, nd, r, own), bf16),
+            pltpu.VMEM((layers - 1, groups, 2, 2, nd, r, own), bf16),
+            pltpu.VMEM((layers - 1, 2, groups, 2, 2, full, own), bf16),
+            pltpu.VMEM((layers - 1, 2, groups, 2, 2, full, own), bf16),
             pltpu.VMEM((layers, 2, groups, 2, r, cols), f32),
             pltpu.VMEM((layers, nd, groups, 2, r, cols), f32),
             pltpu.VMEM((1, rows), jnp.int32),
@@ -782,7 +839,7 @@
             pltpu.VMEM((groups, 2, full, cols), f32),
             pltpu.VMEM((groups, full, own), f32),
             dma((8 + groups + 2 * layers,)),
-            dma((17,)),
+            dma((18,)),
             dma((layers, groups, 2)),
             dma((layers, groups, 2)),
             dma((layers - 1, groups)),
@@ -790,6 +847,7 @@
             dma((groups,)),
             dma((layers - 1, groups)),
             dma((layers - 1, groups)),
+            dma((layers - 1, 2, groups)),
             dma((layers,)),
             dma((layers,)),
             dma((layers,)),

time: 40.3 us -> 39.9 us (0.990)
    pallas_call x1, Pallas kernels: 38.6 us -> 38.2 us  [fused(): pl.pallas_call(functools.partial(fused_kernel, nt, nd, groups), out_shape...]
where the time goes in v4:
time: 39.9 us; the launch traced here: 39.7 us
  Pallas kernels  39.1 us (98%)
  between operations  0.64 us (2%)
    pallas_call x1, Pallas kernels, fused(): pl.pallas_call(functools.partial(fused_kernel, nt, nd, groups), out_shape...  38.2 us
    pallas_call x1, Pallas kernels, fused(): pl.pallas_call(tail_kernel, out_shape=(jax.ShapeDtypeStruct((nd, rows, ow...  0.93 us

profile of v4, /device:TPU:0, one launch (start us, length us, event | category | flops | bytes accessed | tf_op | source)
XLA Modules:
  0.0 39.7 jit_solution(13509035543379958356)
XLA Ops:
  0.6 38.2 %shard_map.139 = (bf16[2,2,4,8,128]{4,3,2,1,0:T(8,128)(2,1)S(1)}, f32[2,2,4,8,512]{4,3,2,1,0:T(8,128)S(1)}, f32[2,2,8,512]{3,2,1,0:T(8,128)S(1)}, bf16[2,2,32,51...) custom-call(bf16[4,32,128]{2,1,0:T(8,128)(2,1)} %bitcast.6, ...), custom_call_target="tpu_custom_call" | custom-call | tf_op jit(solution)/shard_map/pallas_call | solution.py:800
  38.8 0.9 %shard_map.140 = (bf16[4,32,128]{2,1,0:T(8,128)(2,1)}, f32[2,32,512]{2,1,0:T(8,128)}, bf16[2,3,32,512]{3,2,1,0:T(8,128)(2,1)}) custom-call(bf16[2,2,4,8,128]{4,3,2,1,0:T(8,128)(2,1)S(1)} %get-tuple-element.12.mixed, f32[2,2,4,8,512]{4,3,2,1,0:T(8,128)S(1)} %get-tuple-element.13.state, f32[2,2,8,512]{3,2,1,0:T(8,128)S(1)} %get-tuple-element.14.state_m, ...), custom_call_target="tpu_custom_call" | custom-call | tf_op jit(solution)/shard_map/pallas_call | solution.py:875

commit v5 on v4

--- a/solution.py
+++ b/solution.py
@@ -608,11 +608,10 @@
         for h in range(2):
             for k in range(2):
                 xq[l, i, h, k] = whole(l, 1, i, h, k, rq[l, i, h, k])
-        for h in range(2):
-            block, dst = xq.at[l, i, h], xg.at[l + 1, i, h * half + place]
-            for _, peer in tp_near:
-                send(block, dst, "xq", xr.at[l + 1, i, 0], {"tp": peer, "dp": mate})
-            send(block, dst, "xq", xr.at[l + 1, i, 0], {"dp": mate})
+        for where in [{"tp": peer, "dp": mate} for _, peer in tp_near] + [{"dp": mate}]:
+            for h in range(2):
+                block, dst = xq.at[l, i, h], xg.at[l + 1, i, h * half + place]
+                send(block, dst, "xq", xr.at[l + 1, i, 0], where)
 
     def finish(k, i):
         if k == 0:

time: 39.9 us -> 40.1 us (level)
  no operation moved by 1% of the time
where the time goes in v5:
time: 40.1 us; the launch traced here: 39.9 us
  Pallas kernels  39.3 us (98%)
  between operations  0.64 us (2%)
    pallas_call x1, Pallas kernels, fused(): pl.pallas_call(functools.partial(fused_kernel, nt, nd, groups), out_shape...  38.3 us
    pallas_call x1, Pallas kernels, fused(): pl.pallas_call(tail_kernel, out_shape=(jax.ShapeDtypeStruct((nd, rows, ow...  0.93 us

profile of v5, /device:TPU:0, one launch (start us, length us, event | category | flops | bytes accessed | tf_op | source)
XLA Modules:
  0.0 39.9 jit_solution(16108520169585567176)
XLA Ops:
  0.6 38.3 %shard_map.139 = (bf16[2,2,4,8,128]{4,3,2,1,0:T(8,128)(2,1)S(1)}, f32[2,2,4,8,512]{4,3,2,1,0:T(8,128)S(1)}, f32[2,2,8,512]{3,2,1,0:T(8,128)S(1)}, bf16[2,2,32,51...) custom-call(bf16[4,32,128]{2,1,0:T(8,128)(2,1)} %bitcast.6, ...), custom_call_target="tpu_custom_call" | custom-call | tf_op jit(solution)/shard_map/pallas_call | solution.py:799
  39.0 0.9 %shard_map.140 = (bf16[4,32,128]{2,1,0:T(8,128)(2,1)}, f32[2,32,512]{2,1,0:T(8,128)}, bf16[2,3,32,512]{3,2,1,0:T(8,128)(2,1)}) custom-call(bf16[2,2,4,8,128]{4,3,2,1,0:T(8,128)(2,1)S(1)} %get-tuple-element.12.mixed, f32[2,2,4,8,512]{4,3,2,1,0:T(8,128)S(1)} %get-tuple-element.13.state, f32[2,2,8,512]{3,2,1,0:T(8,128)S(1)} %get-tuple-element.14.state_m, ...), custom_call_target="tpu_custom_call" | custom-call | tf_op jit(solution)/shard_map/pallas_call | solution.py:874
